TPU v7x, 512 devices: a whole 4x8x8 slice. The times are simulated.
512 devices in a mesh: fs: 128 (over z, y, core), tp: 4 (over x).
Axes of the slice: x: 4, y: 8, z: 8, core: 2. Of those that a mesh axis runs over, the one named last changes fastest.
Arguments:
- inputs: bfloat16 [98304, 2048], P('fs'), may hold values from -6 to 6
- values_cot: bfloat16 [98304, 2048], P('fs', 'tp'), may hold values from -0.057373047 to 0.057373047
- decay_cot: bfloat16 [98304, 16], P('fs'), may hold values from -0.057373047 to 0.057373047
- factor: bfloat16 [2048, 512], P('fs', 'tp'), may hold values from -0.125 to 0.125
- value_weight: float32 [2048, 2048], P('fs', 'tp'), may hold values from -3 to 3
- lowrank_mean: float32 [512, 2048], P('fs', 'tp'), may hold values from -60 to 60
- lowrank_var: float32 [512, 2048], P('fs', 'tp'), may hold values from 0.3 to 3
- decay_weight: float32 [2048, 16], replicated, may hold values from -3 to 3
- decay_mean: float32 [2048, 16], replicated, may hold values from -6 to 6
- decay_var: float32 [2048, 16], replicated, may hold values from 0.3 to 3
Outputs:
- value_step: float32 [2048, 2048], P('fs', 'tp')
- value_new: float32 [2048, 2048], P('fs', 'tp')
- value_copy: bfloat16 [2048, 2048], P('fs', 'tp')
- mean_new: float32 [512, 2048], P('fs', 'tp')
- var_new: float32 [512, 2048], P('fs', 'tp')
- decay_new: float32 [2048, 16], replicated
- decay_copy: bfloat16 [2048, 16], replicated
- decay_mean_new: float32 [2048, 16], replicated
- decay_var_new: float32 [2048, 16], replicated
All inputs are finite; a program needn't handle non-finite values.
Results may differ from a plain program's by a relative error of at most 0.0042.
Values may be sent and summed in bfloat16 or wider, within the bound.
No kernel may reach another device: no remote copies, remote signals or barrier semaphores. Data moves between devices by JAX's collectives and lax.ppermute only.
A program may use at most 64 MiB of HBM per device.

v0:
```python
import jax
import jax.numpy as jnp
from jax import lax
from jax.sharding import Mesh
from jax.sharding import PartitionSpec as P

W = 2048
R = 512
FS = ("fs_0", "fs_1", "fs_2")


def joined_along(tiles, dim):
    lengths = list(tiles.shape[1:])
    lengths[dim] *= tiles.shape[0]
    return jnp.moveaxis(tiles, 0, dim).reshape(lengths)


def from_everyone(value, axis):
    copies = jnp.broadcast_to(value, (lax.axis_size(axis), *value.shape))
    return lax.all_to_all(copies, axis, split_axis=0, concat_axis=0, tiled=True)


def collect(value, axis, dim):
    return joined_along(from_everyone(value, axis), dim)


def gathered_by_axis(value, axes, dim):
    far, near = axes
    leading = from_everyone(value, far)
    tiles = jnp.swapaxes(from_everyone(leading, near), 0, 1)
    return joined_along(tiles.reshape(-1, *value.shape), dim)


def in_blocks(value, dim, peers):
    lengths = value.shape
    tiles = value.reshape(*lengths[:dim], peers, lengths[dim] // peers, *lengths[dim + 1 :])
    return jnp.moveaxis(tiles, dim, 0)


def summed_on_arrival(value, axis, dim):
    peers = lax.axis_size(axis)
    tiles = lax.all_to_all(in_blocks(value, dim, peers), axis, 0, 0, tiled=True)
    return jnp.sum(tiles.astype(jnp.float32), axis=0)


def summed_rows(value, axes, dim):
    far, near = axes
    tiles = in_blocks(value, dim, lax.axis_size(far))
    nearer = summed_on_arrival(tiles, near, dim + 1)
    arrived = lax.all_to_all(
        nearer.astype(jnp.bfloat16), far, split_axis=0, concat_axis=0, tiled=True
    )
    return arrived.astype(jnp.float32).sum(axis=0)


def taken_together(value, axis):
    return from_everyone(value, axis).sum(axis=0)


def rows_for(lines, peers):
    spare = -len(lines) % peers
    return jnp.pad(lines, [(0, spare)] + [(0, 0)] * (lines.ndim - 1))


def sum_at_owner(value, axis, dim):
    peers = lax.axis_size(axis)
    tiles = lax.all_to_all(in_blocks(value, dim, peers), axis, 0, 0, tiled=True)
    return jnp.sum(tiles, axis=0)


def sum_by_axis(value, axes, dim):
    far, near = axes
    own = sum_at_owner(in_blocks(value, dim, lax.axis_size(far)), near, dim + 1)
    return jnp.sum(lax.all_to_all(own, far, 0, 0, tiled=True), axis=0)


def total_of(value, axes):
    lines = value.reshape(-1, value.shape[-1])
    padded = rows_for(lines, lax.axis_size(axes[0]) * lax.axis_size(axes[1]))
    whole = gathered_by_axis(sum_by_axis(padded, axes, 0), axes, 0)
    return lax.slice_in_dim(whole, 0, len(lines)).reshape(value.shape)


def local(
    inputs,
    values_cot,
    decay_cot,
    factor,
    value_weight,
    lowrank_mean,
    lowrank_var,
    decay_weight,
    decay_mean,
    decay_var,
):
    own_rows = collect(factor, "tp", 1)
    quarter = jnp.dot(
        inputs,
        gathered_by_axis(factor, (("fs_0", "fs_1"), "fs_2"), 0),
        preferred_element_type=jnp.float32,
    ).astype(jnp.bfloat16)
    projected = collect(quarter, "tp", 1)
    lowrank_grad = summed_rows(
        lax.dot_general(
            projected, values_cot, (((0,), (0,)), ((), ())), preferred_element_type=jnp.float32
        ).astype(jnp.bfloat16),
        (("fs_0", "fs_1"), "fs_2"),
        0,
    )
    mean_new = 0.9 * lowrank_mean + 0.1 * lowrank_grad
    var_new = 0.95 * lowrank_var + 0.05 * lowrank_grad * lowrank_grad
    adam_ratio = mean_new / (jnp.sqrt(var_new) + 1e-08)
    full_ratio = gathered_by_axis(adam_ratio, (("fs_0", "fs_1"), "fs_2"), 0)
    squares = taken_together(jnp.sum(full_ratio * full_ratio), "tp")
    root_mean = jnp.sqrt(squares / (R * W) + 1e-06)
    delta = jnp.dot(own_rows.astype(jnp.float32), full_ratio, precision=lax.Precision.HIGHEST)
    value_step = -0.5 / root_mean * delta
    value_new = value_weight + value_step
    value_copy = value_new.astype(jnp.bfloat16)
    decay_part = lax.dot_general(
        inputs, decay_cot, (((0,), (0,)), ((), ())), preferred_element_type=jnp.float32
    )
    decay_grad = total_of(decay_part, (("fs_0", "fs_1"), "fs_2"))
    decay_mean_new = 0.9 * decay_mean + 0.1 * decay_grad
    decay_var_new = 0.95 * decay_var + 0.05 * decay_grad * decay_grad
    decay_new = decay_weight - 0.5 * decay_mean_new / (jnp.sqrt(decay_var_new) + 1e-08)
    decay_copy = decay_new.astype(jnp.bfloat16)
    return (
        value_step,
        value_new,
        value_copy,
        mean_new,
        var_new,
        decay_new,
        decay_copy,
        decay_mean_new,
        decay_var_new,
    )


def solution(mesh):
    split = Mesh(mesh.devices.reshape(8, 8, 2, mesh.shape["tp"]), ("fs_0", "fs_1", "fs_2", "tp"))
    placed = (
        P(FS, None),
        P(FS, "tp"),
        P(FS, None),
        P(FS, "tp"),
        P(FS, "tp"),
        P(FS, "tp"),
        P(FS, "tp"),
        P(),
        P(),
        P(),
    )
    return jax.shard_map(
        local,
        mesh=split,
        in_specs=placed,
        out_specs=(
            P(FS, "tp"),
            P(FS, "tp"),
            P(FS, "tp"),
            P(FS, "tp"),
            P(FS, "tp"),
            P(),
            P(),
            P(),
            P(),
        ),
        check_vma=False,
    )
```

profile of v0, /device:TPU:1, one launch (start us, length us, event | category | flops | bytes accessed | tf_op | source)
XLA Modules:
  0.0 193.9 jit_solution(1163002822927996005)
XLA Ops:
  3.8 2.4 %reshape_reshape.18 = f32[64,2,16,16]{2,1,0,3:T(2,128)} reshape(f32[2048,16]{0,1:T(8,128)S(1)} %fusion.9) | data formatting | bytes 262144 | tf_op jit(solution)/shard_map/reshape;reshape | solution.py:36
  7.8 11.0 %all_to_all.66 = f32[2,1,16384]{2,1,0:T(1,128)} all-to-all(f32[2,1,16384]{2,1,0:T(1,128)S(1)} %reshape.28), channel_id=1, replica_groups=mesh['fs_0'=8,'fs_1'=8,'fs_2'=2,'tp'=4] {'fs_2'}, dimensions={0} | all-to-all | bytes 262144 | tf_op jit(solution)/shard_map/all_to_all | solution.py:67
  19.6 11.0 %all-to-all-start = ((bf16[64,16,128]{2,1,0:T(8,128)(2,1)}), bf16[64,16,128]{2,1,0:T(8,128)(2,1)S(1)}, u32[]{:S(2)}, u32[]{:S(2)}) async-start(bf16[64,16,128]{2,1,0:T(8,128)(2,1)} %broadcast_in_dim.27), calls=%async_computation | async-start | bytes 524288 | tf_op jit(solution)/shard_map/all_to_all | solution.py:20
  37.8 5.9 %all-to-all-done = bf16[64,16,128]{2,1,0:T(8,128)(2,1)S(1)} async-done(((bf16[64,16,128]{2,1,0:T(8,128)(2,1)}), bf16[64,16,128]{2,1,0:T(8,128)(2,1)S(1)}, u32[]{:S(2)}, u32[]{:S(2)}) %all-to-all-start) | async-done | bytes 262176 | tf_op jit(solution)/shard_map/all_to_all | solution.py:20
  43.8 7.2 %all_to_all.67 = bf16[2,64,16,128]{3,2,1,0:T(8,128)(2,1)} all-to-all(bf16[2,64,16,128]{3,2,1,0:T(8,128)(2,1)S(1)} %broadcast_in_dim.28), channel_id=1, replica_groups=mesh['fs_0'=8,'fs_1'=8,'fs_2'=2,'tp'=4] {'fs_2'}, dimensions={0} | all-to-all | bytes 1048576 | tf_op jit(solution)/shard_map/all_to_all | solution.py:20
  51.0 4.6 %all-to-all-start.10 = ((f32[64,1,256]{2,1,0:T(1,128)}), f32[64,1,256]{2,1,0:T(1,128)S(1)}, u32[]{:S(2)}, u32[]{:S(2)}) async-start(f32[64,1,256]{2,1,0:T(1,128)} %reshape.30), calls=%async_computation.10 | async-start | bytes 131072 | tf_op jit(solution)/shard_map/all_to_all | solution.py:74
  59.4 7.3 %all-to-all-done.10 = f32[64,1,256]{2,1,0:T(1,128)S(1)} async-done(((f32[64,1,256]{2,1,0:T(1,128)}), f32[64,1,256]{2,1,0:T(1,128)S(1)}, u32[]{:S(2)}, u32[]{:S(2)}) %all-to-all-start.10) | async-done | bytes 65568 | tf_op jit(solution)/shard_map/all_to_all | solution.py:74
  67.7 4.2 %all-to-all-start.2 = ((bf16[4,768,128]{1,2,0:T(8,128)(2,1)}), bf16[4,768,128]{1,2,0:T(8,128)(2,1)}, u32[]{:S(2)}, u32[]{:S(2)}) async-start(bf16[4,768,128]{1,2,0:T(8,128)(2,1)} %broadcast_in_dim.29), calls=%async_computation.2 | async-start | bytes 1572864 | tf_op jit(solution)/shard_map/all_to_all | solution.py:20
  77.6 4.7 %all-to-all-done.2 = bf16[4,768,128]{1,2,0:T(8,128)(2,1)} async-done(((bf16[4,768,128]{1,2,0:T(8,128)(2,1)}), bf16[4,768,128]{1,2,0:T(8,128)(2,1)}, u32[]{:S(2)}, u32[]{:S(2)}) %all-to-all-start.2) | async-done | bytes 786464 | tf_op jit(solution)/shard_map/all_to_all | solution.py:20
  82.2 2.7 %convolution_convert_fusion = bf16[512,512]{1,0:T(8,128)(2,1)} fusion(bf16[768,512]{0,1:T(8,128)(2,1)} %bitcast.3, bf16[768,512]{1,0:T(8,128)(2,1)} %param.11), kind=kOutput, calls=%fused_computation | convolution fusion | flops 402915328 | bytes 2097152 | tf_op jit(solution)/shard_map/dot_general | solution.py:104
  88.2 7.5 %all_to_all.68 = bf16[2,64,4,512]{3,2,1,0:T(4,128)(2,1)} all-to-all(bf16[2,64,4,512]{3,2,1,0:T(4,128)(2,1)S(1)} %bitcast.54), channel_id=1, replica_groups=mesh['fs_0'=8,'fs_1'=8,'fs_2'=2,'tp'=4] {'fs_2'}, dimensions={0} | all-to-all | bytes 1048576 | tf_op jit(solution)/shard_map/all_to_all | solution.py:42
  95.6 4.9 %all-to-all-start.11 = ((f32[64,1,256]{2,1,0:T(1,128)}), f32[64,1,256]{2,1,0:T(1,128)S(1)}, u32[]{:S(2)}, u32[]{:S(2)}) async-start(f32[64,1,256]{2,1,0:T(1,128)} %reshape.32), calls=%async_computation.11 | async-start | bytes 131072 | tf_op jit(solution)/shard_map/all_to_all | solution.py:20
  102.7 9.0 %all-to-all-done.11 = f32[64,1,256]{2,1,0:T(1,128)S(1)} async-done(((f32[64,1,256]{2,1,0:T(1,128)}), f32[64,1,256]{2,1,0:T(1,128)S(1)}, u32[]{:S(2)}, u32[]{:S(2)}) %all-to-all-start.11) | async-done | bytes 65568 | tf_op jit(solution)/shard_map/all_to_all | solution.py:20
  111.6 5.5 %all-to-all-start.4 = ((bf16[64,4,512]{2,1,0:T(4,128)(2,1)}), bf16[64,4,512]{2,1,0:T(4,128)(2,1)}, u32[]{:S(2)}, u32[]{:S(2)}) async-start(bf16[64,4,512]{2,1,0:T(4,128)(2,1)} %reduce_sum.57), calls=%async_computation.4 | async-start | bytes 524288 | tf_op jit(solution)/shard_map/all_to_all | solution.py:50
  121.1 8.4 %all-to-all-done.4 = bf16[64,4,512]{2,1,0:T(4,128)(2,1)} async-done(((bf16[64,4,512]{2,1,0:T(4,128)(2,1)}), bf16[64,4,512]{2,1,0:T(4,128)(2,1)}, u32[]{:S(2)}, u32[]{:S(2)}) %all-to-all-start.4) | async-done | bytes 262176 | tf_op jit(solution)/shard_map/all_to_all | solution.py:50
  129.5 6.8 %all-to-all-start.12 = ((f32[2,1,16384]{2,1,0:T(1,128)}), f32[2,1,16384]{2,1,0:T(1,128)S(1)}, u32[]{:S(2)}, u32[]{:S(2)}) async-start(f32[2,1,16384]{2,1,0:T(1,128)} %reshape.34), calls=%async_computation.12 | async-start | bytes 262144 | tf_op jit(solution)/shard_map/all_to_all | solution.py:20
  139.5 5.7 %all-to-all-start.5 = ((f32[64,4,512]{2,1,0:T(4,128)}), f32[64,4,512]{2,1,0:T(4,128)}, u32[]{:S(2)}, u32[]{:S(2)}) async-start(f32[64,4,512]{2,1,0:T(4,128)} %broadcast_in_dim.30), calls=%async_computation.5 | async-start | bytes 1048576 | tf_op jit(solution)/shard_map/all_to_all | solution.py:20
  149.4 2.8 %reshape_reshape.19 = f32[2048,16]{0,1:T(8,128)S(1)} reshape(f32[64,2,16,16]{2,1,0,3:T(2,128)} %copy.72) | data formatting | bytes 262144 | tf_op jit(solution)/shard_map/reshape;reshape | solution.py:15
  152.2 10.8 %all-to-all-done.5 = f32[64,4,512]{2,1,0:T(4,128)} async-done(((f32[64,4,512]{2,1,0:T(4,128)}), f32[64,4,512]{2,1,0:T(4,128)}, u32[]{:S(2)}, u32[]{:S(2)}) %all-to-all-start.5) | async-done | bytes 524320 | tf_op jit(solution)/shard_map/all_to_all | solution.py:20
  164.1 5.7 %all_to_all.69 = f32[2,64,4,512]{3,2,1,0:T(4,128)S(1)} all-to-all(f32[2,64,4,512]{3,2,1,0:T(4,128)S(1)} %broadcast_in_dim.31), channel_id=1, replica_groups=mesh['fs_0'=8,'fs_1'=8,'fs_2'=2,'tp'=4] {'fs_2'}, dimensions={0} | all-to-all | bytes 2097152 | tf_op jit(solution)/shard_map/all_to_all | solution.py:20
  172.6 7.1 %all_to_all.70 = f32[4,1,1]{2,1,0:T(1,128)} all-to-all(f32[4,1,1]{2,1,0:T(1,128)S(1)} %broadcast_in_dim.32), channel_id=1, replica_groups=mesh['fs_0'=8,'fs_1'=8,'fs_2'=2,'tp'=4] {'tp'}, dimensions={0} | all-to-all | bytes 32 | tf_op jit(solution)/shard_map/all_to_all | solution.py:20
  180.3 3.3 %all-to-all-start.8 = ((bf16[4,16,128]{2,1,0:T(8,128)(2,1)}), bf16[4,16,128]{2,1,0:T(8,128)(2,1)S(1)}, u32[]{:S(2)}, u32[]{:S(2)}) async-start(bf16[4,16,128]{2,1,0:T(8,128)(2,1)} %broadcast_in_dim.33), calls=%async_computation.8 | async-start | bytes 32768 | tf_op jit(solution)/shard_map/all_to_all | solution.py:20
  185.3 2.4 %copy.66 = f32[64,2,4,512]{3,2,1,0:T(4,128)} copy(f32[64,2,4,512]{3,2,0,1:T(4,128)} %bitcast.50) | data formatting | bytes 2097152 | tf_op jit(solution)/shard_map/transpose | solution.py:30
  187.7 2.6 %reshape_reshape.17 = f32[512,512]{1,0:T(8,128)} reshape(f32[64,2,4,512]{3,2,1,0:T(4,128)} %copy.66) | data formatting | bytes 2097152 | tf_op jit(solution)/shard_map/reshape;reshape | solution.py:15
  (60 shorter events, 49.1 us)
Async XLA Ops:
  0.6 1.9 copy-start
  0.7 18.2 %copy-start.5 = (bf16[16,128]{1,0:T(8,128)(2,1)S(1)}, bf16[16,128]{1,0:T(8,128)(2,1)}, u32[]{:S(2)}) copy-start(bf16[16,128]{1,0:T(8,128)(2,1)} %param.13) | copy-start | bytes 12292
  19.6 24.2 %all-to-all-start = ((bf16[64,16,128]{2,1,0:T(8,128)(2,1)}), bf16[64,16,128]{2,1,0:T(8,128)(2,1)S(1)}, u32[]{:S(2)}, u32[]{:S(2)}) async-start(bf16[64,16,128]{2,1,0:T(8,128)(2,1)} %broadcast_in_dim.27), calls=%async_computation | async-start | bytes 524288 | tf_op jit(solution)/shard_map/all_to_all | solution.py:20
  51.0 15.7 %all-to-all-start.10 = ((f32[64,1,256]{2,1,0:T(1,128)}), f32[64,1,256]{2,1,0:T(1,128)S(1)}, u32[]{:S(2)}, u32[]{:S(2)}) async-start(f32[64,1,256]{2,1,0:T(1,128)} %reshape.30), calls=%async_computation.10 | async-start | bytes 131072 | tf_op jit(solution)/shard_map/all_to_all | solution.py:74
  67.7 14.6 %all-to-all-start.2 = ((bf16[4,768,128]{1,2,0:T(8,128)(2,1)}), bf16[4,768,128]{1,2,0:T(8,128)(2,1)}, u32[]{:S(2)}, u32[]{:S(2)}) async-start(bf16[4,768,128]{1,2,0:T(8,128)(2,1)} %broadcast_in_dim.29), calls=%async_computation.2 | async-start | bytes 1572864 | tf_op jit(solution)/shard_map/all_to_all | solution.py:20
  86.9 50.4 %copy-start.7 = (f32[4,512]{1,0:T(4,128)S(1)}, f32[4,512]{1,0:T(4,128)}, u32[]{:S(2)}) copy-start(f32[4,512]{1,0:T(4,128)} %param.16) | copy-start | bytes 24580
  95.6 16.0 %all-to-all-start.11 = ((f32[64,1,256]{2,1,0:T(1,128)}), f32[64,1,256]{2,1,0:T(1,128)S(1)}, u32[]{:S(2)}, u32[]{:S(2)}) async-start(f32[64,1,256]{2,1,0:T(1,128)} %reshape.32), calls=%async_computation.11 | async-start | bytes 131072 | tf_op jit(solution)/shard_map/all_to_all | solution.py:20
  111.6 17.8 %all-to-all-start.4 = ((bf16[64,4,512]{2,1,0:T(4,128)(2,1)}), bf16[64,4,512]{2,1,0:T(4,128)(2,1)}, u32[]{:S(2)}, u32[]{:S(2)}) async-start(bf16[64,4,512]{2,1,0:T(4,128)(2,1)} %reduce_sum.57), calls=%async_computation.4 | async-start | bytes 524288 | tf_op jit(solution)/shard_map/all_to_all | solution.py:50
  129.5 9.2 %all-to-all-start.12 = ((f32[2,1,16384]{2,1,0:T(1,128)}), f32[2,1,16384]{2,1,0:T(1,128)S(1)}, u32[]{:S(2)}, u32[]{:S(2)}) async-start(f32[2,1,16384]{2,1,0:T(1,128)} %reshape.34), calls=%async_computation.12 | async-start | bytes 262144 | tf_op jit(solution)/shard_map/all_to_all | solution.py:20
  139.5 23.4 %all-to-all-start.5 = ((f32[64,4,512]{2,1,0:T(4,128)}), f32[64,4,512]{2,1,0:T(4,128)}, u32[]{:S(2)}, u32[]{:S(2)}) async-start(f32[64,4,512]{2,1,0:T(4,128)} %broadcast_in_dim.30), calls=%async_computation.5 | async-start | bytes 1048576 | tf_op jit(solution)/shard_map/all_to_all | solution.py:20
  149.4 34.2 %copy-start.2 = (f32[2048,16]{0,1:T(8,128)S(1)}, f32[2048,16]{0,1:T(8,128)}, u32[]{:S(2)}) copy-start(f32[2048,16]{0,1:T(8,128)} %param.17) | copy-start | bytes 393220
  149.4 34.2 %copy-start.3 = (f32[2048,16]{0,1:T(8,128)S(1)}, f32[2048,16]{0,1:T(8,128)}, u32[]{:S(2)}) copy-start(f32[2048,16]{0,1:T(8,128)} %param.18) | copy-start | bytes 393220
  169.8 1.0 copy-start.1
  180.3 11.3 %all-to-all-start.8 = ((bf16[4,16,128]{2,1,0:T(8,128)(2,1)}), bf16[4,16,128]{2,1,0:T(8,128)(2,1)S(1)}, u32[]{:S(2)}, u32[]{:S(2)}) async-start(bf16[4,16,128]{2,1,0:T(8,128)(2,1)} %broadcast_in_dim.33), calls=%async_computation.8 | async-start | bytes 32768 | tf_op jit(solution)/shard_map/all_to_all | solution.py:20
  185.3 5.0 %copy-start.6 = (f32[4,1,1]{2,1,0:T(1,128)S(1)}, f32[4,1,1]{2,1,0:T(1,128)}, u32[]{:S(2)}) copy-start(f32[4,1,1]{2,1,0:T(1,128)} %all_to_all.70) | copy-start | bytes 52
  185.3 6.3 %copy-start.4 = (f32[16,512]{1,0:T(8,128)S(1)}, f32[16,512]{1,0:T(8,128)}, u32[]{:S(2)}) copy-start(f32[16,512]{1,0:T(8,128)} %param.14) | copy-start | bytes 98308
where the time goes:
time: 197 us; the launch traced here: 194 us
  waiting for transfers between devices  46 us (23%)
  starting transfers between devices  45.9 us (23%)
  local copies, waits for them, and re-layouts  39.5 us (20%)
  blocking collectives  38.4 us (19%)
  other arithmetic  14.6 us (7%)
  matrix products  7.95 us (4%)
    all_to_all x6, starting transfers between devices, from_everyone(): return lax.all_to_all(copies, axis, split_axis=0, concat_axis=0, tiled=True)  35.8 us
    all_to_all x6, waiting for transfers between devices, from_everyone(): return lax.all_to_all(copies, axis, split_axis=0, concat_axis=0, tiled=True)  30.3 us
    all_to_all x3, blocking collectives, from_everyone(): return lax.all_to_all(copies, axis, split_axis=0, concat_axis=0, tiled=True)  20 us
    unnamed x26, local copies, waits for them, and re-layouts  12.4 us
    all_to_all x1, blocking collectives, sum_at_owner(): tiles = lax.all_to_all(in_blocks(value, dim, peers), axis, 0, 0, tiled=True)  11 us
    all_to_all x1, waiting for transfers between devices, summed_rows(): lax.all_to_all(nearer.astype(jnp.bfloat16), far, split_axis=0, concat_axi...  8.4 us
    all_to_all x1, blocking collectives, summed_on_arrival(): tiles = lax.all_to_all(in_blocks(value, dim, peers), axis, 0, 0, tiled=True)  7.45 us
    all_to_all x1, waiting for transfers between devices, sum_by_axis(): return jnp.sum(lax.all_to_all(own, far, 0, 0, tiled=True), axis=0)  7.29 us
  transfers between devices with their start and end apart: 8, of which 6 were waited for; matrix products, arithmetic and copies ran while one was open for 20% of the time, Pallas kernels for 0%

commit v1 on v0

v1 whole, which is shorter than its diff:
```python
import functools

import jax
import jax.numpy as jnp
from jax import lax
from jax.experimental import pallas as pl
from jax.experimental.pallas import tpu as pltpu
from jax.sharding import Mesh
from jax.sharding import PartitionSpec as P

D = 2048
W = 2048
R = 512
H = 16
FS = ("z", "y", "c")
PLANE = ("z", "y")
CHIPS = 64
SWAP = [(0, 1), (1, 0)]
BF = jnp.bfloat16
F32 = jnp.float32
VMEM = pl.BlockSpec(memory_space=pltpu.VMEM)


def call(body, outs, count, flops, moved, scratch=()):
    return pl.pallas_call(
        body,
        out_shape=outs,
        in_specs=[VMEM] * count,
        out_specs=jax.tree.map(lambda _: VMEM, outs),
        scratch_shapes=list(scratch),
        compiler_params=pltpu.CompilerParams(vmem_limit_bytes=12 << 20),
        cost_estimate=pl.CostEstimate(flops=flops, bytes_accessed=moved, transcendentals=0),
    )


def shape(dims, dtype):
    return jax.ShapeDtypeStruct(dims, dtype)


def split_pair(pair, axis):
    total = pair + pltpu.roll(pair, 4, axis)
    high = total.astype(BF).astype(F32)
    row = lax.broadcasted_iota(jnp.int32, pair.shape, axis)
    return jnp.where(row < 4, high, total - high)


def decay_body(cot_ref, x_ref, out_ref, rows):
    part = jnp.dot(cot_ref[...], x_ref[...], preferred_element_type=F32)
    high = part.astype(BF).astype(F32)
    low = part - high
    for b in range(D // 128):
        at = (b // 4) * 8 + b % 4
        lanes = slice(b * 128, (b + 1) * 128)
        rows[pl.ds(at, H, stride=32), :] = high[:, lanes]
        rows[pl.ds(at + 4, H, stride=32), :] = low[:, lanes]
    out_ref[...] = rows[...].astype(BF).reshape(CHIPS, 8, 128)


def project_body(x_ref, near_ref, far_ref, own_ref, out_ref, whole):
    core = lax.axis_index("c")
    whole[:, pl.ds(core, 1)] = near_ref[...].reshape(CHIPS, 1, 16, 128)
    whole[:, pl.ds(1 - core, 1)] = far_ref[...].reshape(CHIPS, 1, 16, 128)
    part = jnp.dot(
        x_ref[...], whole[...].reshape(D, 128), preferred_element_type=F32
    ).astype(BF)
    a = lax.broadcasted_iota(jnp.int32, (128, 128), 0)
    lane = lax.broadcasted_iota(jnp.int32, (128, 128), 1)
    half = jnp.where(a < 64, 1 - core, core)
    source = (a & 15) * 8 + half * 4 + ((a >> 4) & 3)
    order = jnp.where(lane == source, 1.0, 0.0).astype(BF)
    turned = lax.dot_general(
        order, part, (((1,), (1,)), ((), ())), preferred_element_type=F32
    ).astype(BF)
    out_ref[0:128, :] = turned
    out_ref[128:144, :] = jnp.zeros((16, 768), BF)
    out_ref[128:144, 0:128] = own_ref[...]


def gradient_body(half, p_ref, v_ref, dec_ref, out_ref, rows):
    for q in range(4):
        part = jnp.dot(
            p_ref[q, half * 64 : half * 64 + 64, :], v_ref[...], preferred_element_type=F32
        )
        for i in range(4):
            for cb in range(4):
                rows[pl.ds(q * 256 + cb * 4 + i, 16, stride=16), :] = part[
                    i * 16 : i * 16 + 16, cb * 128 : cb * 128 + 128
                ]
    out_ref[:, 0:16, :] = rows[...].astype(BF).reshape(CHIPS, 16, 128)
    out_ref[:, 16:24, :] = dec_ref[...]


def pair_body(own_ref, peer_ref, out_ref):
    out_ref[:, 0:16, :] = (
        own_ref[:, 0:16, :].astype(F32) + peer_ref[:, 0:16, :].astype(F32)
    ).astype(BF)
    dec = own_ref[:, 16:24, :].astype(F32) + peer_ref[:, 16:24, :].astype(F32)
    out_ref[:, 16:24, :] = split_pair(dec, 1).astype(BF)


def moment_body(got_ref, mean_ref, var_ref, out_ref, mean_out, var_out, mean_s, var_s):
    for cb in range(4):
        lanes = slice(cb * 128, cb * 128 + 128)
        mean_s[cb * 4 : cb * 4 + 4, :] = mean_ref[:, lanes]
        var_s[cb * 4 : cb * 4 + 4, :] = var_ref[:, lanes]
    grad = jnp.sum(got_ref[:, 0:16, :].astype(F32), axis=0)
    dec = jnp.sum(got_ref[:, 16:24, :].astype(F32), axis=0)
    mean_new = 0.9 * mean_s[...] + 0.1 * grad
    var_new = 0.95 * var_s[...] + 0.05 * grad * grad
    ratio = mean_new / (jnp.sqrt(var_new) + 1e-08)
    mean_s[...] = mean_new
    var_s[...] = var_new
    for cb in range(4):
        lanes = slice(cb * 128, cb * 128 + 128)
        mean_out[:, lanes] = mean_s[cb * 4 : cb * 4 + 4, :]
        var_out[:, lanes] = var_s[cb * 4 : cb * 4 + 4, :]
    out_ref[:, 0:16, :] = jnp.broadcast_to(ratio.astype(BF)[None], (CHIPS, 16, 128))
    out_ref[:, 16:24, :] = jnp.broadcast_to(
        split_pair(dec, 0).astype(BF)[None], (CHIPS, 8, 128)
    )


def spread_body(p_ref, out_ref):
    core = lax.axis_index("c")
    lane = lax.broadcasted_iota(jnp.int32, (128, 256), 0)
    k = lax.broadcasted_iota(jnp.int32, (128, 256), 1)
    column = (lax.broadcasted_iota(jnp.int32, (16, 256), 1) >> 2) & 3
    for side in range(2):
        half = core if side == 0 else 1 - core
        pick = jnp.where(lane == (k >> 4) * 8 + half * 4 + (k & 3), 1.0, 0.0).astype(BF)
        for q in range(4):
            rows = jnp.dot(p_ref[q, 128:144, 0:128], pick, preferred_element_type=F32)
            for cb in range(4):
                out_ref[side, cb * 16 : cb * 16 + 16, q * 256 : q * 256 + 256] = jnp.where(
                    column == cb, rows, 0.0
                ).astype(BF)


def decay_update_body(
    got_ref, weight_ref, mean_ref, var_ref, new_out, copy_out, mean_out, var_out, rows
):
    dec = got_ref[:, 16:24, :].astype(F32)
    rows[...] = (dec + pltpu.roll(dec, 4, 1)).reshape(CHIPS * 8, 128)
    for b in range(D // 128):
        lanes = slice(b * 128, (b + 1) * 128)
        grad = rows[pl.ds((b // 4) * 8 + b % 4, H, stride=32), :]
        mean_new = 0.9 * mean_ref[:, lanes] + 0.1 * grad
        var_new = 0.95 * var_ref[:, lanes] + 0.05 * grad * grad
        new = weight_ref[:, lanes] - 0.5 * mean_new / (jnp.sqrt(var_new) + 1e-08)
        mean_out[:, lanes] = mean_new
        var_out[:, lanes] = var_new
        new_out[:, lanes] = new
        copy_out[:, lanes] = new.astype(BF)


def squares_body(near_ref, far_ref, out_ref):
    near = near_ref[:, 0:16, :].astype(F32)
    far = far_ref[:, 0:16, :].astype(F32)
    sums = jnp.sum(near * near + far * far, axis=0)
    sums = sums[0:8] + sums[8:16]
    out_ref[...] = jnp.broadcast_to(sums[None], (4, 8, 128))


def product_body(rows_ref, near_ref, far_ref, out_ref):
    near = near_ref[:, 0:16, :].reshape(CHIPS * 16, 128)
    far = far_ref[:, 0:16, :].reshape(CHIPS * 16, 128)
    got = jnp.dot(rows_ref[0], near, preferred_element_type=F32) + jnp.dot(
        rows_ref[1], far, preferred_element_type=F32
    )
    for cb in range(4):
        out_ref[:, cb * 128 : cb * 128 + 128] = got[cb * 16 : cb * 16 + 16]


def step_body(squares_ref, delta_ref, weight_ref, step_out, new_out, copy_out):
    root_mean = jnp.sqrt(jnp.sum(squares_ref[...]) / (R * W) + 1e-06)
    step = -0.5 / root_mean * delta_ref[...]
    new = weight_ref[...] + step
    step_out[...] = step
    new_out[...] = new
    copy_out[...] = new.astype(BF)


def local(
    inputs,
    values_cot,
    decay_cot,
    factor,
    value_weight,
    lowrank_mean,
    lowrank_var,
    decay_weight,
    decay_mean,
    decay_var,
):
    chunk = shape((CHIPS, 24, 128), BF)
    near = lax.all_to_all(
        jnp.broadcast_to(factor, (CHIPS, 16, 128)), PLANE, 0, 0, tiled=True
    )
    decay_rows = call(
        decay_body,
        shape((CHIPS, 8, 128), BF),
        2,
        2 * 768 * D * H,
        4 << 20,
        [pltpu.VMEM((512, 128), F32)],
    )(decay_cot.T, inputs)
    far = lax.ppermute(near, "c", SWAP)
    quarter = call(
        project_body,
        shape((144, 768), BF),
        4,
        2 * 768 * D * 128,
        4 << 20,
        [pltpu.VMEM((CHIPS, 2, 16, 128), BF)],
    )(inputs, near, far, factor)
    projected = lax.all_gather(quarter, "x")

    def gradient(half):
        return call(
            functools.partial(gradient_body, half),
            chunk,
            3,
            2 * 768 * 256 * 512,
            2 << 20,
            [pltpu.VMEM((CHIPS * 16, 128), F32)],
        )(projected, values_cot, decay_rows)

    peer = lax.ppermute(gradient(0), "c", SWAP)
    paired = call(pair_body, chunk, 2, 400000, 1 << 20)(gradient(1), peer)
    arrived = lax.all_to_all(paired, PLANE, 0, 0, tiled=True)
    rows = call(spread_body, shape((2, 64, 1024), BF), 1, 8 * 2 * 16 * 128 * 256, 1 << 20)(
        projected
    )
    ratio, mean_new, var_new = call(
        moment_body,
        (chunk, shape((4, 512), F32), shape((4, 512), F32)),
        3,
        400000,
        1 << 20,
        [pltpu.VMEM((16, 128), F32)] * 2,
    )(arrived, lowrank_mean, lowrank_var)
    near = lax.all_to_all(ratio, PLANE, 0, 0, tiled=True)
    far = lax.ppermute(near, "c", SWAP)
    state = shape((H, D), F32)
    decay_new, decay_copy, decay_mean_new, decay_var_new = call(
        decay_update_body,
        (state, shape((H, D), BF), state, state),
        4,
        400000,
        1 << 20,
        [pltpu.VMEM((512, 128), F32)],
    )(near, decay_weight.T, decay_mean.T, decay_var.T)
    squares = call(squares_body, shape((4, 8, 128), F32), 2, 400000, 1 << 20)(near, far)
    squares = lax.all_to_all(squares, "x", 0, 0, tiled=True)
    delta = call(
        product_body, shape((16, 512), F32), 3, 2 * 64 * 2048 * 128, 1 << 20
    )(rows, near, far)
    block = shape((16, 512), F32)
    value_step, value_new, value_copy = call(
        step_body, (block, block, shape((16, 512), BF)), 3, 40000, 100000
    )(squares, delta, value_weight)
    return (
        value_step,
        value_new,
        value_copy,
        mean_new,
        var_new,
        decay_new.T,
        decay_copy.T,
        decay_mean_new.T,
        decay_var_new.T,
    )


def solution(mesh):
    split = Mesh(mesh.devices.reshape(8, 8, 2, mesh.shape["tp"]), ("z", "y", "c", "x"))
    placed = (
        P(FS, None),
        P(FS, "x"),
        P(FS, None),
        P(FS, "x"),
        P(FS, "x"),
        P(FS, "x"),
        P(FS, "x"),
        P(),
        P(),
        P(),
    )
    return jax.shard_map(
        local,
        mesh=split,
        in_specs=placed,
        out_specs=(P(FS, "x"),) * 5 + (P(),) * 4,
        check_vma=False,
    )
```

time: 197 us -> 117 us (0.59); the launches traced: 194 us -> 117 us
  blocking collectives: 38.4 us -> 81.2 us
  waiting for transfers between devices: 46 us -> 4.75 us
  local copies, waits for them, and re-layouts: 39.5 us -> 3.45 us
  starting transfers between devices: 45.9 us -> 19.3 us
  other arithmetic: 14.6 us -> 0 us
  matrix products: 7.95 us -> 0 us
  Pallas kernels: 0 us -> 7.09 us
    all_to_all x8 -> x1, waiting for transfers between devices: 46 us -> 2.82 us  [local(): squares = lax.all_to_all(squares, 'x', 0, 0, tiled=True)]
    all_to_all x8 -> x1, starting transfers between devices: 45.9 us -> 4.13 us  [local(): squares = lax.all_to_all(squares, 'x', 0, 0, tiled=True)]
    all_to_all x5 -> x3, blocking collectives: 38.4 us -> 68.9 us  [the longest x1 29.8 us: local(): lax.all_to_all(jnp.broadcast_to(factor, (CHIPS, 16, 128)), PLANE, 0, 0, t...]
    ppermute x0 -> x3, starting transfers between devices: none -> 15.2 us  [the longest x2 10.8 us: local(): far = lax.ppermute(near, 'c', SWAP)]
    all_gather x0 -> x1, blocking collectives: none -> 12.3 us  [local(): projected = lax.all_gather(quarter, 'x')]
    another operation x5 -> x0, local copies, waits for them, and re-layouts: 11 us -> none  [the longest x3 5.59 us: in_blocks(): value.reshape(*lengths[:dim], peers, lengths[dim] // peers, *lengths[dim...]
    unnamed x26 -> x20, local copies, waits for them, and re-layouts: 12.4 us -> 2.67 us
    dot_general x4 -> x0, matrix products: 7.95 us -> none  [the longest x1 2.74 us: local(): lax.dot_general(projected, values_cot, (((0,), (0,)), ((), ())), preferre...]
  transfers between devices with their start and end apart: 8 -> 4, of which waited for: 6 -> 3; matrix products, arithmetic and copies ran while one was open for 20% -> 0% of each run, Pallas kernels for 0% -> 2%
where the time goes in v1:
time: 117 us
  blocking collectives  81.2 us (69%)
  starting transfers between devices  19.3 us (16%)
  Pallas kernels  7.09 us (6%)
  waiting for transfers between devices  4.75 us (4%)
  local copies, waits for them, and re-layouts  3.45 us (3%)
    all_to_all x1, blocking collectives, local(): lax.all_to_all(jnp.broadcast_to(factor, (CHIPS, 16, 128)), PLANE, 0, 0, t...  29.8 us
    all_to_all x1, blocking collectives, local(): near = lax.all_to_all(ratio, PLANE, 0, 0, tiled=True)  20.1 us
    all_to_all x1, blocking collectives, local(): arrived = lax.all_to_all(paired, PLANE, 0, 0, tiled=True)  19.1 us
    all_gather x1, blocking collectives, local(): projected = lax.all_gather(quarter, 'x')  12.3 us
    ppermute x2, starting transfers between devices, local(): far = lax.ppermute(near, 'c', SWAP)  10.8 us
    ppermute x1, starting transfers between devices, local(): peer = lax.ppermute(gradient(0), 'c', SWAP)  4.35 us
    all_to_all x1, starting transfers between devices, local(): squares = lax.all_to_all(squares, 'x', 0, 0, tiled=True)  4.13 us
    all_to_all x1, waiting for transfers between devices, local(): squares = lax.all_to_all(squares, 'x', 0, 0, tiled=True)  2.82 us
  transfers between devices with their start and end apart: 4, of which 3 were waited for; matrix products, arithmetic and copies ran while one was open for 0% of the time, Pallas kernels for 2%

profile of v1, /device:TPU:1, one launch (start us, length us, event | category | flops | bytes accessed | tf_op | source)
XLA Modules:
  0.0 116.7 jit_solution(10339720972181770580)
XLA Ops:
  0.7 0.8 broadcast_in_dim.3
  1.4 29.8 %all_to_all.20.near_ref = bf16[64,16,128]{2,1,0:T(8,128)(2,1)S(1)} all-to-all(bf16[64,16,128]{2,1,0:T(8,128)(2,1)S(1)} %broadcast_in_dim.3), channel_id=1, replica_groups=mesh['z'=8,'y'=8,'c'=2,'x'=4] {'z','y'}, dimensions={0} | all-to-all | bytes 524288 | tf_op jit(solution)/shard_map/all_to_all | solution.py:196
  31.2 5.0 %collective-permute-start = (bf16[64,16,128]{2,1,0:T(8,128)(2,1)S(1)}, bf16[64,16,128]{2,1,0:T(8,128)(2,1)S(1)}, u32[]{:S(2)}, u32[]{:S(2)}) collective-permute-start(bf16[64,16,128]{2,1,0:T(8,128)(2,1)S(1)} %all_to_all.20.near_ref), channel_id=1, source_target_pairs={{0,4},{4,0},{1,5},{5,1},{2,6},{6,2},{3,7},{7,3},{8,12},{12,8},{9,1... | collective-permute-start | bytes 786440 | tf_op jit(solution)/shard_map/ppermute | solution.py:207
  36.2 1.9 %copy-done = bf16[768,2048]{1,0:T(8,128)(2,1)S(1)} copy-done((bf16[768,2048]{1,0:T(8,128)(2,1)S(1)}, bf16[768,2048]{1,0:T(8,128)(2,1)}, u32[]{:S(2)}) %copy-start) | copy-done | bytes 3145752
  38.1 0.7 copy-done.6
  38.8 0.7 shard_map.170.dec_ref
  39.5 1.2 %shard_map.169 = bf16[144,768]{1,0:T(8,128)(2,1)S(1)} custom-call(bf16[768,2048]{1,0:T(8,128)(2,1)S(1)} %copy-done, bf16[64,16,128]{2,1,0:T(8,128)(2,1)S(1)} %all_to_all.20.near_ref, bf16[64,16,128]{2,1,0:T(8,128)(2,1)S(1)} %collective-permute-done.far_ref, bf16[16,128]{1,0:T(8,128)(2,1)S(1)} %copy-done.7), custom_call_target="tpu_custom_call" | custom-call | flops 402653184 | bytes 4194304 | tf_op jit(solution)/shard_map/pallas_call | solution.py:208
  40.8 12.3 %all-gather = bf16[576,768]{1,0:T(8,128)(2,1)S(1)} all-gather(bf16[144,768]{1,0:T(8,128)(2,1)S(1)} %shard_map.169), channel_id=2, replica_groups=mesh['z'=8,'y'=8,'c'=2,'x'=4] {'x'}, dimensions={0}, use_global_device_ids=true | all-gather | bytes 1105920 | tf_op jit(solution)/shard_map/all_gather | solution.py:216
  53.0 0.7 shard_map.172
  53.8 4.3 %collective-permute-start.1 = (bf16[64,24,128]{2,1,0:T(8,128)(2,1)S(1)}, bf16[64,24,128]{2,1,0:T(8,128)(2,1)S(1)}, u32[]{:S(2)}, u32[]{:S(2)}) collective-permute-start(bf16[64,24,128]{2,1,0:T(8,128)(2,1)S(1)} %shard_map.172), channel_id=1, source_target_pairs={{0,4},{4,0},{1,5},{5,1},{2,6},{6,2},{3,7},{7,3},{8,12},{12,8},{9,1... | collective-permute-start | bytes 1179656 | tf_op jit(solution)/shard_map/ppermute | solution.py:228
  58.2 0.7 shard_map.171.own_ref
  58.9 0.6 collective-permute-done.1.peer_ref
  59.7 19.1 %all_to_all.21.got_ref = bf16[64,24,128]{2,1,0:T(8,128)(2,1)S(1)} all-to-all(bf16[64,24,128]{2,1,0:T(8,128)(2,1)S(1)} %shard_map.173), channel_id=1, replica_groups=mesh['z'=8,'y'=8,'c'=2,'x'=4] {'z','y'}, dimensions={0} | all-to-all | bytes 786432 | tf_op jit(solution)/shard_map/all_to_all | solution.py:230
  78.8 0.7 shard_map.174
  79.4 20.1 %all_to_all.22.near_ref.got_ref = bf16[64,24,128]{2,1,0:T(8,128)(2,1)S(1)} all-to-all(bf16[64,24,128]{2,1,0:T(8,128)(2,1)S(1)} %get-tuple-element.19), channel_id=1, replica_groups=mesh['z'=8,'y'=8,'c'=2,'x'=4] {'z','y'}, dimensions={0} | all-to-all | bytes 786432 | tf_op jit(solution)/shard_map/all_to_all | solution.py:242
  99.5 5.9 %collective-permute-start.2 = (bf16[64,24,128]{2,1,0:T(8,128)(2,1)S(1)}, bf16[64,24,128]{2,1,0:T(8,128)(2,1)S(1)}, u32[]{:S(2)}, u32[]{:S(2)}) collective-permute-start(bf16[64,24,128]{2,1,0:T(8,128)(2,1)S(1)} %all_to_all.22.near_ref.got_ref), channel_id=1, source_target_pairs={{0,4},{4,0},{1,5},{5,1},{2,6},{6,2},{3,7},{7,3},{8,12},{12,8},{9,1... | collective-permute-start | bytes 1179656 | tf_op jit(solution)/shard_map/ppermute | solution.py:243
  105.4 1.3 %collective-permute-done.2.far_ref = bf16[64,24,128]{2,1,0:T(8,128)(2,1)S(1)} collective-permute-done((bf16[64,24,128]{2,1,0:T(8,128)(2,1)S(1)}, bf16[64,24,128]{2,1,0:T(8,128)(2,1)S(1)}, u32[]{:S(2)}, u32[]{:S(2)}) %collective-permute-start.2) | collective-permute-done | bytes 393248 | tf_op jit(solution)/shard_map/ppermute | solution.py:243
  106.7 0.7 shard_map.175
  107.5 4.1 %all-to-all-start.3 = ((f32[4,8,128]{2,1,0:T(8,128)}), f32[4,8,128]{2,1,0:T(8,128)S(1)}, u32[]{:S(2)}, u32[]{:S(2)}) async-start(f32[4,8,128]{2,1,0:T(8,128)} %shard_map.175), calls=%async_computation.3 | async-start | bytes 32768 | tf_op jit(solution)/shard_map/all_to_all | solution.py:254
  111.6 0.2 shard_map.176.rows_ref
  111.8 0.9 shard_map.179
  112.8 0.2 shard_map.177.delta_ref
  113.0 2.8 %all-to-all-done.3.squares_ref = f32[4,8,128]{2,1,0:T(8,128)S(1)} async-done(((f32[4,8,128]{2,1,0:T(8,128)}), f32[4,8,128]{2,1,0:T(8,128)S(1)}, u32[]{:S(2)}, u32[]{:S(2)}) %all-to-all-start.3) | async-done | bytes 16416 | tf_op jit(solution)/shard_map/all_to_all | solution.py:254
  115.8 0.8 shard_map.178
  (20 shorter events, 0.2 us)
Async XLA Ops:
  0.6 38.8 %copy-start.7 = (bf16[16,128]{1,0:T(8,128)(2,1)S(1)}, bf16[16,128]{1,0:T(8,128)(2,1)}, u32[]{:S(2)}) copy-start(bf16[16,128]{1,0:T(8,128)(2,1)} %own_ref.1) | copy-start | bytes 12292
  31.2 8.3 %collective-permute-start = (bf16[64,16,128]{2,1,0:T(8,128)(2,1)S(1)}, bf16[64,16,128]{2,1,0:T(8,128)(2,1)S(1)}, u32[]{:S(2)}, u32[]{:S(2)}) collective-permute-start(bf16[64,16,128]{2,1,0:T(8,128)(2,1)S(1)} %all_to_all.20.near_ref), channel_id=1, source_target_pairs={{0,4},{4,0},{1,5},{5,1},{2,6},{6,2},{3,7},{7,3},{8,12},{12,8},{9,1... | collective-permute-start | bytes 786440 | tf_op jit(solution)/shard_map/ppermute | solution.py:207
  36.2 1.9 %copy-start = (bf16[768,2048]{1,0:T(8,128)(2,1)S(1)}, bf16[768,2048]{1,0:T(8,128)(2,1)}, u32[]{:S(2)}) copy-start(bf16[768,2048]{1,0:T(8,128)(2,1)} %x_ref.3) | copy-start | bytes 9437188
  38.1 0.7 copy-start.6
  39.5 13.6 %copy-start.1 = (bf16[768,512]{1,0:T(8,128)(2,1)S(1)}, bf16[768,512]{1,0:T(8,128)(2,1)}, u32[]{:S(2)}) copy-start(bf16[768,512]{1,0:T(8,128)(2,1)} %v_ref.3) | copy-start | bytes 2359300
  53.0 25.7 %copy-start.8 = (f32[4,512]{1,0:T(4,128)S(1)}, f32[4,512]{1,0:T(4,128)}, u32[]{:S(2)}) copy-start(f32[4,512]{1,0:T(4,128)} %mean_ref.1) | copy-start | bytes 24580
  53.0 25.7 %copy-start.9 = (f32[4,512]{1,0:T(4,128)S(1)}, f32[4,512]{1,0:T(4,128)}, u32[]{:S(2)}) copy-start(f32[4,512]{1,0:T(4,128)} %var_ref.1) | copy-start | bytes 24580
  53.8 58.0 %copy-start.2 = (f32[2048,16]{0,1:T(8,128)S(1)}, f32[2048,16]{0,1:T(8,128)}, u32[]{:S(2)}) copy-start(f32[2048,16]{0,1:T(8,128)} %param.17) | copy-start | bytes 393220
  53.8 58.0 %copy-start.3 = (f32[2048,16]{0,1:T(8,128)S(1)}, f32[2048,16]{0,1:T(8,128)}, u32[]{:S(2)}) copy-start(f32[2048,16]{0,1:T(8,128)} %param.18) | copy-start | bytes 393220
  53.8 58.0 %copy-start.4 = (f32[2048,16]{0,1:T(8,128)S(1)}, f32[2048,16]{0,1:T(8,128)}, u32[]{:S(2)}) copy-start(f32[2048,16]{0,1:T(8,128)} %param.19) | copy-start | bytes 393220
  53.8 5.7 %collective-permute-start.1 = (bf16[64,24,128]{2,1,0:T(8,128)(2,1)S(1)}, bf16[64,24,128]{2,1,0:T(8,128)(2,1)S(1)}, u32[]{:S(2)}, u32[]{:S(2)}) collective-permute-start(bf16[64,24,128]{2,1,0:T(8,128)(2,1)S(1)} %shard_map.172), channel_id=1, source_target_pairs={{0,4},{4,0},{1,5},{5,1},{2,6},{6,2},{3,7},{7,3},{8,12},{12,8},{9,1... | collective-permute-start | bytes 1179656 | tf_op jit(solution)/shard_map/ppermute | solution.py:228
  59.6 56.2 %copy-start.5 = (f32[16,512]{1,0:T(8,128)S(1)}, f32[16,512]{1,0:T(8,128)}, u32[]{:S(2)}) copy-start(f32[16,512]{1,0:T(8,128)} %weight_ref.1) | copy-start | bytes 98308
  99.5 7.2 %collective-permute-start.2 = (bf16[64,24,128]{2,1,0:T(8,128)(2,1)S(1)}, bf16[64,24,128]{2,1,0:T(8,128)(2,1)S(1)}, u32[]{:S(2)}, u32[]{:S(2)}) collective-permute-start(bf16[64,24,128]{2,1,0:T(8,128)(2,1)S(1)} %all_to_all.22.near_ref.got_ref), channel_id=1, source_target_pairs={{0,4},{4,0},{1,5},{5,1},{2,6},{6,2},{3,7},{7,3},{8,12},{12,8},{9,1... | collective-permute-start | bytes 1179656 | tf_op jit(solution)/shard_map/ppermute | solution.py:243
  107.5 8.3 %all-to-all-start.3 = ((f32[4,8,128]{2,1,0:T(8,128)}), f32[4,8,128]{2,1,0:T(8,128)S(1)}, u32[]{:S(2)}, u32[]{:S(2)}) async-start(f32[4,8,128]{2,1,0:T(8,128)} %shard_map.175), calls=%async_computation.3 | async-start | bytes 32768 | tf_op jit(solution)/shard_map/all_to_all | solution.py:254

commit v2 on v1

--- a/solution.py
+++ b/solution.py
@@ -153,12 +153,11 @@
         copy_out[:, lanes] = new.astype(BF)
 
 
-def squares_body(near_ref, far_ref, out_ref):
+def squares_body(near_ref, out_ref):
     near = near_ref[:, 0:16, :].astype(F32)
-    far = far_ref[:, 0:16, :].astype(F32)
-    sums = jnp.sum(near * near + far * far, axis=0)
+    sums = jnp.sum(near * near, axis=0)
     sums = sums[0:8] + sums[8:16]
-    out_ref[...] = jnp.broadcast_to(sums[None], (4, 8, 128))
+    out_ref[...] = jnp.broadcast_to(sums[None], (8, 8, 128))
 
 
 def product_body(rows_ref, near_ref, far_ref, out_ref):
@@ -204,6 +203,7 @@
         4 << 20,
         [pltpu.VMEM((512, 128), F32)],
     )(decay_cot.T, inputs)
+    near, decay_rows = lax.optimization_barrier((near, decay_rows))
     far = lax.ppermute(near, "c", SWAP)
     quarter = call(
         project_body,
@@ -250,8 +250,8 @@
         1 << 20,
         [pltpu.VMEM((512, 128), F32)],
     )(near, decay_weight.T, decay_mean.T, decay_var.T)
-    squares = call(squares_body, shape((4, 8, 128), F32), 2, 400000, 1 << 20)(near, far)
-    squares = lax.all_to_all(squares, "x", 0, 0, tiled=True)
+    squares = call(squares_body, shape((8, 8, 128), F32), 1, 400000, 1 << 20)(near)
+    squares = lax.all_to_all(squares, ("c", "x"), 0, 0, tiled=True)
     delta = call(
         product_body, shape((16, 512), F32), 3, 2 * 64 * 2048 * 128, 1 << 20
     )(rows, near, far)

time: 117 us -> 116 us (level)
  blocking collectives: 81.2 us -> 51.6 us
  starting transfers between devices: 19.3 us -> 37 us
  waiting for transfers between devices: 4.75 us -> 14.8 us
    all_to_all x1 -> x0, blocking collectives: 29.8 us -> none  [local(): lax.all_to_all(jnp.broadcast_to(factor, (CHIPS, 16, 128)), PLANE, 0, 0, t...]
    all_to_all x1 -> x2, starting transfers between devices: 4.13 us -> 21.8 us  [the longest x1 17.1 us: local(): lax.all_to_all(jnp.broadcast_to(factor, (CHIPS, 16, 128)), PLANE, 0, 0, t...]
    all_to_all x1 -> x2, waiting for transfers between devices: 2.82 us -> 13.1 us  [the longest x1 9.54 us: local(): lax.all_to_all(jnp.broadcast_to(factor, (CHIPS, 16, 128)), PLANE, 0, 0, t...]
    unnamed x20 -> x22, local copies, waits for them, and re-layouts: 2.67 us -> 2.67 us
  transfers between devices with their start and end apart: 4 -> 5, of which waited for: 3 -> 4; matrix products, arithmetic and copies ran while one was open for 0% -> 0% of each run, Pallas kernels for 2% -> 3%
where the time goes in v2:
time: 116 us; the launch traced here: 115 us
  blocking collectives  51.6 us (44%)
  starting transfers between devices  37 us (32%)
  waiting for transfers between devices  14.8 us (13%)
  Pallas kernels  7.04 us (6%)
  local copies, waits for them, and re-layouts  4.15 us (4%)
    all_to_all x1, blocking collectives, local(): near = lax.all_to_all(ratio, PLANE, 0, 0, tiled=True)  20.1 us
    all_to_all x1, blocking collectives, local(): arrived = lax.all_to_all(paired, PLANE, 0, 0, tiled=True)  19.1 us
    all_to_all x1, starting transfers between devices, local(): lax.all_to_all(jnp.broadcast_to(factor, (CHIPS, 16, 128)), PLANE, 0, 0, t...  17.1 us
    all_gather x1, blocking collectives, local(): projected = lax.all_gather(quarter, 'x')  12.4 us
    ppermute x2, starting transfers between devices, local(): far = lax.ppermute(near, 'c', SWAP)  11 us
    all_to_all x1, waiting for transfers between devices, local(): lax.all_to_all(jnp.broadcast_to(factor, (CHIPS, 16, 128)), PLANE, 0, 0, t...  9.54 us
    all_to_all x1, starting transfers between devices, local(): squares = lax.all_to_all(squares, ('c', 'x'), 0, 0, tiled=True)  4.66 us
    ppermute x1, starting transfers between devices, local(): peer = lax.ppermute(gradient(0), 'c', SWAP)  4.21 us
  transfers between devices with their start and end apart: 5, of which 4 were waited for; matrix products, arithmetic and copies ran while one was open for 0% of the time, Pallas kernels for 3%

profile of v2, /device:TPU:1, one launch (start us, length us, event | category | flops | bytes accessed | tf_op | source)
XLA Modules:
  0.0 115.4 jit_solution(5560028982419623609)
XLA Ops:
  0.7 1.5 %broadcast_in_dim.3 = bf16[64,16,128]{2,1,0:T(8,128)(2,1)} broadcast(bf16[16,128]{1,0:T(8,128)(2,1)} %own_ref.1), dimensions={1,2} | broadcast | bytes 266240 | tf_op jit(solution)/shard_map/broadcast_in_dim | solution.py:196
  2.1 17.1 %all-to-all-start = ((bf16[64,16,128]{2,1,0:T(8,128)(2,1)}), bf16[64,16,128]{2,1,0:T(8,128)(2,1)S(1)}, u32[]{:S(2)}, u32[]{:S(2)}) async-start(bf16[64,16,128]{2,1,0:T(8,128)(2,1)} %broadcast_in_dim.3), calls=%async_computation | async-start | bytes 524288 | tf_op jit(solution)/shard_map/all_to_all | solution.py:195
  19.3 1.9 %copy-done = bf16[768,2048]{1,0:T(8,128)(2,1)S(1)} copy-done((bf16[768,2048]{1,0:T(8,128)(2,1)S(1)}, bf16[768,2048]{1,0:T(8,128)(2,1)}, u32[]{:S(2)}) %copy-start) | copy-done | bytes 3145752
  21.2 0.7 copy-done.7
  21.9 0.7 shard_map.169.dec_ref
  22.6 9.5 %all-to-all-done.near_ref = bf16[64,16,128]{2,1,0:T(8,128)(2,1)S(1)} async-done(((bf16[64,16,128]{2,1,0:T(8,128)(2,1)}), bf16[64,16,128]{2,1,0:T(8,128)(2,1)S(1)}, u32[]{:S(2)}, u32[]{:S(2)}) %all-to-all-start) | async-done | bytes 262176 | tf_op jit(solution)/shard_map/all_to_all | solution.py:195
  32.1 5.1 %collective-permute-start = (bf16[64,16,128]{2,1,0:T(8,128)(2,1)S(1)}, bf16[64,16,128]{2,1,0:T(8,128)(2,1)S(1)}, u32[]{:S(2)}, u32[]{:S(2)}) collective-permute-start(bf16[64,16,128]{2,1,0:T(8,128)(2,1)S(1)} %all-to-all-done.near_ref), channel_id=1, source_target_pairs={{0,4},{4,0},{1,5},{5,1},{2,6},{6,2},{3,7},{7,3},{8,12},{12,8},{9,1... | collective-permute-start | bytes 786440 | tf_op jit(solution)/shard_map/ppermute | solution.py:207
  37.2 1.1 collective-permute-done.far_ref
  38.4 1.3 %shard_map.170 = bf16[144,768]{1,0:T(8,128)(2,1)S(1)} custom-call(bf16[768,2048]{1,0:T(8,128)(2,1)S(1)} %copy-done.1, bf16[64,16,128]{2,1,0:T(8,128)(2,1)S(1)} %all-to-all-done.near_ref, bf16[64,16,128]{2,1,0:T(8,128)(2,1)S(1)} %collective-permute-done.far_ref, bf16[16,128]{1,0:T(8,128)(2,1)S(1)} %copy-done.8), custom_call_target="tpu_custom_call" | custom-call | flops 402653184 | bytes 4194304 | tf_op jit(solution)/shard_map/pallas_call | solution.py:208
  39.6 12.4 %all-gather = bf16[576,768]{1,0:T(8,128)(2,1)S(1)} all-gather(bf16[144,768]{1,0:T(8,128)(2,1)S(1)} %shard_map.170), channel_id=2, replica_groups=mesh['z'=8,'y'=8,'c'=2,'x'=4] {'x'}, dimensions={0}, use_global_device_ids=true | all-gather | bytes 1105920 | tf_op jit(solution)/shard_map/all_gather | solution.py:216
  52.0 0.7 shard_map.172
  52.8 4.2 %collective-permute-start.1 = (bf16[64,24,128]{2,1,0:T(8,128)(2,1)S(1)}, bf16[64,24,128]{2,1,0:T(8,128)(2,1)S(1)}, u32[]{:S(2)}, u32[]{:S(2)}) collective-permute-start(bf16[64,24,128]{2,1,0:T(8,128)(2,1)S(1)} %shard_map.172), channel_id=1, source_target_pairs={{0,4},{4,0},{1,5},{5,1},{2,6},{6,2},{3,7},{7,3},{8,12},{12,8},{9,1... | collective-permute-start | bytes 1179656 | tf_op jit(solution)/shard_map/ppermute | solution.py:228
  57.0 0.7 shard_map.171.own_ref
  57.7 0.6 collective-permute-done.1.peer_ref
  58.5 19.1 %all_to_all.20.got_ref = bf16[64,24,128]{2,1,0:T(8,128)(2,1)S(1)} all-to-all(bf16[64,24,128]{2,1,0:T(8,128)(2,1)S(1)} %shard_map.173), channel_id=1, replica_groups=mesh['z'=8,'y'=8,'c'=2,'x'=4] {'z','y'}, dimensions={0} | all-to-all | bytes 786432 | tf_op jit(solution)/shard_map/all_to_all | solution.py:230
  77.6 0.7 shard_map.174
  78.3 20.1 %all_to_all.21.near_ref.got_ref = bf16[64,24,128]{2,1,0:T(8,128)(2,1)S(1)} all-to-all(bf16[64,24,128]{2,1,0:T(8,128)(2,1)S(1)} %get-tuple-element.23), channel_id=1, replica_groups=mesh['z'=8,'y'=8,'c'=2,'x'=4] {'z','y'}, dimensions={0} | all-to-all | bytes 786432 | tf_op jit(solution)/shard_map/all_to_all | solution.py:242
  98.4 5.9 %collective-permute-start.2 = (bf16[64,24,128]{2,1,0:T(8,128)(2,1)S(1)}, bf16[64,24,128]{2,1,0:T(8,128)(2,1)S(1)}, u32[]{:S(2)}, u32[]{:S(2)}) collective-permute-start(bf16[64,24,128]{2,1,0:T(8,128)(2,1)S(1)} %all_to_all.21.near_ref.got_ref), channel_id=1, source_target_pairs={{0,4},{4,0},{1,5},{5,1},{2,6},{6,2},{3,7},{7,3},{8,12},{12,8},{9,1... | collective-permute-start | bytes 1179656 | tf_op jit(solution)/shard_map/ppermute | solution.py:243
  104.3 0.7 shard_map.175
  104.9 4.7 %all-to-all-start.3 = ((f32[8,8,128]{2,1,0:T(8,128)}), f32[8,8,128]{2,1,0:T(8,128)S(1)}, u32[]{:S(2)}, u32[]{:S(2)}) async-start(f32[8,8,128]{2,1,0:T(8,128)} %shard_map.175), calls=%async_computation.3 | async-start | bytes 65536 | tf_op jit(solution)/shard_map/all_to_all | solution.py:254
  109.8 0.9 shard_map.179
  110.8 0.2 shard_map.177.delta_ref
  111.0 3.5 %all-to-all-done.3.squares_ref = f32[8,8,128]{2,1,0:T(8,128)S(1)} async-done(((f32[8,8,128]{2,1,0:T(8,128)}), f32[8,8,128]{2,1,0:T(8,128)S(1)}, u32[]{:S(2)}, u32[]{:S(2)}) %all-to-all-start.3) | async-done | bytes 32800 | tf_op jit(solution)/shard_map/all_to_all | solution.py:254
  114.5 0.8 shard_map.178
  (23 shorter events, 0.4 us)
Async XLA Ops:
  0.6 37.7 %copy-start.8 = (bf16[16,128]{1,0:T(8,128)(2,1)S(1)}, bf16[16,128]{1,0:T(8,128)(2,1)}, u32[]{:S(2)}) copy-start(bf16[16,128]{1,0:T(8,128)(2,1)} %own_ref.1) | copy-start | bytes 12292
  2.1 30.0 %all-to-all-start = ((bf16[64,16,128]{2,1,0:T(8,128)(2,1)}), bf16[64,16,128]{2,1,0:T(8,128)(2,1)S(1)}, u32[]{:S(2)}, u32[]{:S(2)}) async-start(bf16[64,16,128]{2,1,0:T(8,128)(2,1)} %broadcast_in_dim.3), calls=%async_computation | async-start | bytes 524288 | tf_op jit(solution)/shard_map/all_to_all | solution.py:195
  19.3 1.9 %copy-start = (bf16[768,2048]{1,0:T(8,128)(2,1)S(1)}, bf16[768,2048]{1,0:T(8,128)(2,1)}, u32[]{:S(2)}) copy-start(bf16[768,2048]{1,0:T(8,128)(2,1)} %x_ref.3) | copy-start | bytes 9437188
  21.2 0.7 copy-start.7
  21.9 16.5 %copy-start.1 = (bf16[768,2048]{1,0:T(8,128)(2,1)S(1)}, bf16[768,2048]{1,0:T(8,128)(2,1)}, u32[]{:S(2)}) copy-start(bf16[768,2048]{1,0:T(8,128)(2,1)} %x_ref.3) | copy-start | bytes 9437188
  32.1 19.9 %copy-start.2 = (bf16[768,512]{1,0:T(8,128)(2,1)S(1)}, bf16[768,512]{1,0:T(8,128)(2,1)}, u32[]{:S(2)}) copy-start(bf16[768,512]{1,0:T(8,128)(2,1)} %v_ref.3) | copy-start | bytes 2359300
  32.1 6.2 %collective-permute-start = (bf16[64,16,128]{2,1,0:T(8,128)(2,1)S(1)}, bf16[64,16,128]{2,1,0:T(8,128)(2,1)S(1)}, u32[]{:S(2)}, u32[]{:S(2)}) collective-permute-start(bf16[64,16,128]{2,1,0:T(8,128)(2,1)S(1)} %all-to-all-done.near_ref), channel_id=1, source_target_pairs={{0,4},{4,0},{1,5},{5,1},{2,6},{6,2},{3,7},{7,3},{8,12},{12,8},{9,1... | collective-permute-start | bytes 786440 | tf_op jit(solution)/shard_map/ppermute | solution.py:207
  52.0 25.6 %copy-start.9 = (f32[4,512]{1,0:T(4,128)S(1)}, f32[4,512]{1,0:T(4,128)}, u32[]{:S(2)}) copy-start(f32[4,512]{1,0:T(4,128)} %mean_ref.1) | copy-start | bytes 24580
  52.0 25.6 %copy-start.10 = (f32[4,512]{1,0:T(4,128)S(1)}, f32[4,512]{1,0:T(4,128)}, u32[]{:S(2)}) copy-start(f32[4,512]{1,0:T(4,128)} %var_ref.1) | copy-start | bytes 24580
  52.8 57.0 %copy-start.3 = (f32[2048,16]{0,1:T(8,128)S(1)}, f32[2048,16]{0,1:T(8,128)}, u32[]{:S(2)}) copy-start(f32[2048,16]{0,1:T(8,128)} %param.17) | copy-start | bytes 393220
  52.8 57.0 %copy-start.4 = (f32[2048,16]{0,1:T(8,128)S(1)}, f32[2048,16]{0,1:T(8,128)}, u32[]{:S(2)}) copy-start(f32[2048,16]{0,1:T(8,128)} %param.18) | copy-start | bytes 393220
  52.8 57.0 %copy-start.5 = (f32[2048,16]{0,1:T(8,128)S(1)}, f32[2048,16]{0,1:T(8,128)}, u32[]{:S(2)}) copy-start(f32[2048,16]{0,1:T(8,128)} %param.19) | copy-start | bytes 393220
  52.8 5.5 %collective-permute-start.1 = (bf16[64,24,128]{2,1,0:T(8,128)(2,1)S(1)}, bf16[64,24,128]{2,1,0:T(8,128)(2,1)S(1)}, u32[]{:S(2)}, u32[]{:S(2)}) collective-permute-start(bf16[64,24,128]{2,1,0:T(8,128)(2,1)S(1)} %shard_map.172), channel_id=1, source_target_pairs={{0,4},{4,0},{1,5},{5,1},{2,6},{6,2},{3,7},{7,3},{8,12},{12,8},{9,1... | collective-permute-start | bytes 1179656 | tf_op jit(solution)/shard_map/ppermute | solution.py:228
  57.7 56.8 %copy-start.6 = (f32[16,512]{1,0:T(8,128)S(1)}, f32[16,512]{1,0:T(8,128)}, u32[]{:S(2)}) copy-start(f32[16,512]{1,0:T(8,128)} %weight_ref.1) | copy-start | bytes 98308
  98.4 12.4 %collective-permute-start.2 = (bf16[64,24,128]{2,1,0:T(8,128)(2,1)S(1)}, bf16[64,24,128]{2,1,0:T(8,128)(2,1)S(1)}, u32[]{:S(2)}, u32[]{:S(2)}) collective-permute-start(bf16[64,24,128]{2,1,0:T(8,128)(2,1)S(1)} %all_to_all.21.near_ref.got_ref), channel_id=1, source_target_pairs={{0,4},{4,0},{1,5},{5,1},{2,6},{6,2},{3,7},{7,3},{8,12},{12,8},{9,1... | collective-permute-start | bytes 1179656 | tf_op jit(solution)/shard_map/ppermute | solution.py:243
  104.9 9.6 %all-to-all-start.3 = ((f32[8,8,128]{2,1,0:T(8,128)}), f32[8,8,128]{2,1,0:T(8,128)S(1)}, u32[]{:S(2)}, u32[]{:S(2)}) async-start(f32[8,8,128]{2,1,0:T(8,128)} %shard_map.175), calls=%async_computation.3 | async-start | bytes 65536 | tf_op jit(solution)/shard_map/all_to_all | solution.py:254

commit v3 on v2

--- a/solution.py
+++ b/solution.py
@@ -1,5 +1,3 @@
-import functools
-
 import jax
 import jax.numpy as jnp
 from jax import lax
@@ -56,6 +54,11 @@
     out_ref[...] = rows[...].astype(BF).reshape(CHIPS, 8, 128)
 
 
+def pair_body(own_ref, peer_ref, out_ref):
+    dec = own_ref[...].astype(F32) + peer_ref[...].astype(F32)
+    out_ref[...] = split_pair(dec, 1).astype(BF)
+
+
 def project_body(x_ref, near_ref, far_ref, own_ref, out_ref, whole):
     core = lax.axis_index("c")
     whole[:, pl.ds(core, 1)] = near_ref[...].reshape(CHIPS, 1, 16, 128)
@@ -65,37 +68,33 @@
     ).astype(BF)
     a = lax.broadcasted_iota(jnp.int32, (128, 128), 0)
     lane = lax.broadcasted_iota(jnp.int32, (128, 128), 1)
-    half = jnp.where(a < 64, 1 - core, core)
-    source = (a & 15) * 8 + half * 4 + ((a >> 4) & 3)
+    source = (a & 15) * 8 + (a >> 6) * 4 + ((a >> 4) & 3)
     order = jnp.where(lane == source, 1.0, 0.0).astype(BF)
     turned = lax.dot_general(
         order, part, (((1,), (1,)), ((), ())), preferred_element_type=F32
     ).astype(BF)
-    out_ref[0:128, :] = turned
-    out_ref[128:144, :] = jnp.zeros((16, 768), BF)
-    out_ref[128:144, 0:128] = own_ref[...]
-
-
-def gradient_body(half, p_ref, v_ref, dec_ref, out_ref, rows):
+    for to in range(8):
+        out_ref[to, 0:64, :] = turned[(to // 4) * 64 : (to // 4) * 64 + 64]
+        out_ref[to, 64:72, :] = jnp.zeros((8, 768), BF)
+        out_ref[to, 64:72, 0:128] = own_ref[0:8]
+        out_ref[to, 64:72, 128:256] = own_ref[8:16]
+
+
+def gradient_body(p_ref, own_ref, peer_ref, dec_ref, out_ref, rows):
+    core = lax.axis_index("c")
+    own = p_ref[pl.ds(core * 4, 4), 0:64, :].reshape(256, 768)
+    peer = p_ref[pl.ds((1 - core) * 4, 4), 0:64, :].reshape(256, 768)
+    part = jnp.dot(own, own_ref[...], preferred_element_type=F32) + jnp.dot(
+        peer, peer_ref[...], preferred_element_type=F32
+    )
     for q in range(4):
-        part = jnp.dot(
-            p_ref[q, half * 64 : half * 64 + 64, :], v_ref[...], preferred_element_type=F32
-        )
         for i in range(4):
             for cb in range(4):
                 rows[pl.ds(q * 256 + cb * 4 + i, 16, stride=16), :] = part[
-                    i * 16 : i * 16 + 16, cb * 128 : cb * 128 + 128
+                    q * 64 + i * 16 : q * 64 + i * 16 + 16, cb * 128 : cb * 128 + 128
                 ]
     out_ref[:, 0:16, :] = rows[...].astype(BF).reshape(CHIPS, 16, 128)
     out_ref[:, 16:24, :] = dec_ref[...]
-
-
-def pair_body(own_ref, peer_ref, out_ref):
-    out_ref[:, 0:16, :] = (
-        own_ref[:, 0:16, :].astype(F32) + peer_ref[:, 0:16, :].astype(F32)
-    ).astype(BF)
-    dec = own_ref[:, 16:24, :].astype(F32) + peer_ref[:, 16:24, :].astype(F32)
-    out_ref[:, 16:24, :] = split_pair(dec, 1).astype(BF)
 
 
 def moment_body(got_ref, mean_ref, var_ref, out_ref, mean_out, var_out, mean_s, var_s):
@@ -129,7 +128,13 @@
         half = core if side == 0 else 1 - core
         pick = jnp.where(lane == (k >> 4) * 8 + half * 4 + (k & 3), 1.0, 0.0).astype(BF)
         for q in range(4):
-            rows = jnp.dot(p_ref[q, 128:144, 0:128], pick, preferred_element_type=F32)
+            own = jnp.concatenate(
+                [
+                    p_ref[core * 4 + q, 64:72, 0:128].astype(F32),
+                    p_ref[core * 4 + q, 64:72, 128:256].astype(F32),
+                ]
+            ).astype(BF)
+            rows = jnp.dot(own, pick, preferred_element_type=F32)
             for cb in range(4):
                 out_ref[side, cb * 16 : cb * 16 + 16, q * 256 : q * 256 + 256] = jnp.where(
                     column == cb, rows, 0.0
@@ -203,30 +208,29 @@
         4 << 20,
         [pltpu.VMEM((512, 128), F32)],
     )(decay_cot.T, inputs)
-    near, decay_rows = lax.optimization_barrier((near, decay_rows))
+    values_peer = lax.ppermute(values_cot, "c", SWAP)
+    decay_rows = call(pair_body, shape((CHIPS, 8, 128), BF), 2, 400000, 1 << 20)(
+        decay_rows, lax.ppermute(decay_rows, "c", SWAP)
+    )
+    near, decay_rows, values_peer = lax.optimization_barrier((near, decay_rows, values_peer))
     far = lax.ppermute(near, "c", SWAP)
-    quarter = call(
+    parts = call(
         project_body,
-        shape((144, 768), BF),
+        shape((8, 72, 768), BF),
         4,
         2 * 768 * D * 128,
         4 << 20,
         [pltpu.VMEM((CHIPS, 2, 16, 128), BF)],
     )(inputs, near, far, factor)
-    projected = lax.all_gather(quarter, "x")
-
-    def gradient(half):
-        return call(
-            functools.partial(gradient_body, half),
-            chunk,
-            3,
-            2 * 768 * 256 * 512,
-            2 << 20,
-            [pltpu.VMEM((CHIPS * 16, 128), F32)],
-        )(projected, values_cot, decay_rows)
-
-    peer = lax.ppermute(gradient(0), "c", SWAP)
-    paired = call(pair_body, chunk, 2, 400000, 1 << 20)(gradient(1), peer)
+    projected = lax.all_to_all(parts, ("c", "x"), 0, 0, tiled=True)
+    paired = call(
+        gradient_body,
+        chunk,
+        4,
+        2 * 1536 * 256 * 512,
+        3 << 20,
+        [pltpu.VMEM((CHIPS * 16, 128), F32)],
+    )(projected, values_cot, values_peer, decay_rows)
     arrived = lax.all_to_all(paired, PLANE, 0, 0, tiled=True)
     rows = call(spread_body, shape((2, 64, 1024), BF), 1, 8 * 2 * 16 * 128 * 256, 1 << 20)(
         projected

time: 116 us -> 118 us (1.017)
  blocking collectives: 51.6 us -> 56.9 us
  waiting for transfers between devices: 14.8 us -> 12.5 us
  starting transfers between devices: 37 us -> 35.6 us
    all_to_all x0 -> x1, blocking collectives: none -> 17.8 us  [local(): projected = lax.all_to_all(parts, ('c', 'x'), 0, 0, tiled=True)]
    all_gather x1 -> x0, blocking collectives: 12.4 us -> none  [local(): projected = lax.all_gather(quarter, 'x')]
    ppermute x1 -> x2, starting transfers between devices: 4.21 us -> 11.1 us  [the longest x1 8.75 us: local(): values_peer = lax.ppermute(values_cot, 'c', SWAP)]
    all_to_all x1, starting transfers between devices: 17.1 us -> 11 us  [local(): lax.all_to_all(jnp.broadcast_to(factor, (CHIPS, 16, 128)), PLANE, 0, 0, t...]
    all_to_all x1, waiting for transfers between devices: 9.54 us -> 6.82 us  [local(): lax.all_to_all(jnp.broadcast_to(factor, (CHIPS, 16, 128)), PLANE, 0, 0, t...]
    all_to_all x1, starting transfers between devices: 4.66 us -> 3.29 us  [local(): squares = lax.all_to_all(squares, ('c', 'x'), 0, 0, tiled=True)]
    pallas_call x4 -> x3, Pallas kernels: 2.84 us -> 3.23 us  [the longest x1 1.89 us: local(): call(gradient_body, chunk, 4, 2 * 1536 * 256 * 512, 3 << 20, [pltpu.VMEM(...]
  transfers between devices with their start and end apart: 5 -> 6, of which waited for: 4 -> 4; matrix products, arithmetic and copies ran while one was open for 0% -> 1% of each run, Pallas kernels for 3% -> 2%
where the time goes in v3:
time: 118 us; the launch traced here: 117 us
  blocking collectives  56.9 us (48%)
  starting transfers between devices  35.6 us (30%)
  waiting for transfers between devices  12.5 us (11%)
  Pallas kernels  7.44 us (6%)
  local copies, waits for them, and re-layouts  4.08 us (3%)
    all_to_all x1, blocking collectives, local(): near = lax.all_to_all(ratio, PLANE, 0, 0, tiled=True)  19.8 us
    all_to_all x1, blocking collectives, local(): arrived = lax.all_to_all(paired, PLANE, 0, 0, tiled=True)  19.2 us
    all_to_all x1, blocking collectives, local(): projected = lax.all_to_all(parts, ('c', 'x'), 0, 0, tiled=True)  17.8 us
    all_to_all x1, starting transfers between devices, local(): lax.all_to_all(jnp.broadcast_to(factor, (CHIPS, 16, 128)), PLANE, 0, 0, t...  11 us
    ppermute x2, starting transfers between devices, local(): far = lax.ppermute(near, 'c', SWAP)  10.2 us
    ppermute x1, starting transfers between devices, local(): values_peer = lax.ppermute(values_cot, 'c', SWAP)  8.75 us
    all_to_all x1, waiting for transfers between devices, local(): lax.all_to_all(jnp.broadcast_to(factor, (CHIPS, 16, 128)), PLANE, 0, 0, t...  6.82 us
    all_to_all x1, waiting for transfers between devices, local(): squares = lax.all_to_all(squares, ('c', 'x'), 0, 0, tiled=True)  3.49 us
  transfers between devices with their start and end apart: 6, of which 4 were waited for; matrix products, arithmetic and copies ran while one was open for 1% of the time, Pallas kernels for 2%

profile of v3, /device:TPU:1, one launch (start us, length us, event | category | flops | bytes accessed | tf_op | source)
XLA Modules:
  0.0 117.3 jit_solution(14935589276283230399)
XLA Ops:
  0.7 8.8 %collective-permute-start.1 = (bf16[768,512]{1,0:T(8,128)(2,1)}, bf16[768,512]{1,0:T(8,128)(2,1)}, u32[]{:S(2)}, u32[]{:S(2)}) collective-permute-start(bf16[768,512]{1,0:T(8,128)(2,1)} %own_ref.3), channel_id=1, source_target_pairs={{0,4},{4,0},{1,5},{5,1},{2,6},{6,2},{3,7},{7,3},{8,12},{12,8},{9,1... | collective-permute-start | bytes 2359304 | tf_op jit(solution)/shard_map/ppermute | solution.py:211
  9.4 1.4 %broadcast_in_dim.3 = bf16[64,16,128]{2,1,0:T(8,128)(2,1)} broadcast(bf16[16,128]{1,0:T(8,128)(2,1)} %own_ref.2), dimensions={1,2} | broadcast | bytes 266240 | tf_op jit(solution)/shard_map/broadcast_in_dim | solution.py:201
  10.8 11.0 %all-to-all-start = ((bf16[64,16,128]{2,1,0:T(8,128)(2,1)}), bf16[64,16,128]{2,1,0:T(8,128)(2,1)S(1)}, u32[]{:S(2)}, u32[]{:S(2)}) async-start(bf16[64,16,128]{2,1,0:T(8,128)(2,1)} %broadcast_in_dim.3), calls=%async_computation | async-start | bytes 524288 | tf_op jit(solution)/shard_map/all_to_all | solution.py:200
  21.8 1.9 %copy-done = bf16[768,2048]{1,0:T(8,128)(2,1)S(1)} copy-done((bf16[768,2048]{1,0:T(8,128)(2,1)S(1)}, bf16[768,2048]{1,0:T(8,128)(2,1)}, u32[]{:S(2)}) %copy-start) | copy-done | bytes 3145752
  23.7 0.7 copy-done.7
  24.4 0.7 shard_map.169.own_ref
  25.1 2.3 %collective-permute-start = (bf16[64,8,128]{2,1,0:T(8,128)(2,1)S(1)}, bf16[64,8,128]{2,1,0:T(8,128)(2,1)S(1)}, u32[]{:S(2)}, u32[]{:S(2)}) collective-permute-start(bf16[64,8,128]{2,1,0:T(8,128)(2,1)S(1)} %shard_map.169.own_ref), channel_id=1, source_target_pairs={{0,4},{4,0},{1,5},{5,1},{2,6},{6,2},{3,7},{7,3},{8,12},{12,8},{9,1... | collective-permute-start | bytes 393224 | tf_op jit(solution)/shard_map/ppermute | solution.py:213
  27.4 1.0 collective-permute-done.peer_ref
  28.6 6.8 %all-to-all-done.near_ref = bf16[64,16,128]{2,1,0:T(8,128)(2,1)S(1)} async-done(((bf16[64,16,128]{2,1,0:T(8,128)(2,1)}), bf16[64,16,128]{2,1,0:T(8,128)(2,1)S(1)}, u32[]{:S(2)}, u32[]{:S(2)}) %all-to-all-start) | async-done | bytes 262176 | tf_op jit(solution)/shard_map/all_to_all | solution.py:200
  35.4 4.3 %collective-permute-start.2 = (bf16[64,16,128]{2,1,0:T(8,128)(2,1)S(1)}, bf16[64,16,128]{2,1,0:T(8,128)(2,1)S(1)}, u32[]{:S(2)}, u32[]{:S(2)}) collective-permute-start(bf16[64,16,128]{2,1,0:T(8,128)(2,1)S(1)} %all-to-all-done.near_ref), channel_id=1, source_target_pairs={{0,4},{4,0},{1,5},{5,1},{2,6},{6,2},{3,7},{7,3},{8,12},{12,8},{9,1... | collective-permute-start | bytes 786440 | tf_op jit(solution)/shard_map/ppermute | solution.py:216
  39.7 1.1 collective-permute-done.2.far_ref
  40.8 1.3 %shard_map.171 = bf16[8,72,768]{2,1,0:T(8,128)(2,1)S(1)} custom-call(bf16[768,2048]{1,0:T(8,128)(2,1)S(1)} %copy-done.1, bf16[64,16,128]{2,1,0:T(8,128)(2,1)S(1)} %all-to-all-done.near_ref, bf16[64,16,128]{2,1,0:T(8,128)(2,1)S(1)} %collective-permute-done.2.far_ref, bf16[16,128]{1,0:T(8,128)(2,1)S(1)} %copy-done.8), custom_call_target="tpu_custom_call" | custom-call | flops 402653184 | bytes 4194304 | tf_op jit(solution)/shard_map/pallas_call | solution.py:217
  42.1 17.8 %all_to_all.25.p_ref = bf16[8,72,768]{2,1,0:T(8,128)(2,1)S(1)} all-to-all(bf16[8,72,768]{2,1,0:T(8,128)(2,1)S(1)} %shard_map.171), channel_id=1, replica_groups=mesh['z'=8,'y'=8,'c'=2,'x'=4] {'c','x'}, dimensions={0} | all-to-all | bytes 1769472 | tf_op jit(solution)/shard_map/all_to_all | solution.py:225
  59.9 1.9 %shard_map.172 = bf16[64,24,128]{2,1,0:T(8,128)(2,1)S(1)} custom-call(bf16[8,72,768]{2,1,0:T(8,128)(2,1)S(1)} %all_to_all.25.p_ref, bf16[768,512]{1,0:T(8,128)(2,1)S(1)} %copy-done.2, bf16[768,512]{1,0:T(8,128)(2,1)} %collective-permute-done.1.peer_ref, bf16[64,8,128]{2,1,0:T(8,128)(2,1)S(1)} %shard_map.170.dec_ref), custom_call_target="tpu_custom_call" | custom-call | flops 402653184 | bytes 3145728 | tf_op jit(solution)/shard_map/pallas_call | solution.py:226
  61.9 19.2 %all_to_all.26.got_ref = bf16[64,24,128]{2,1,0:T(8,128)(2,1)S(1)} all-to-all(bf16[64,24,128]{2,1,0:T(8,128)(2,1)S(1)} %shard_map.172), channel_id=1, replica_groups=mesh['z'=8,'y'=8,'c'=2,'x'=4] {'z','y'}, dimensions={0} | all-to-all | bytes 786432 | tf_op jit(solution)/shard_map/all_to_all | solution.py:234
  81.1 0.7 shard_map.173
  81.7 19.8 %all_to_all.27.near_ref.got_ref = bf16[64,24,128]{2,1,0:T(8,128)(2,1)S(1)} all-to-all(bf16[64,24,128]{2,1,0:T(8,128)(2,1)S(1)} %get-tuple-element.25), channel_id=1, replica_groups=mesh['z'=8,'y'=8,'c'=2,'x'=4] {'z','y'}, dimensions={0} | all-to-all | bytes 786432 | tf_op jit(solution)/shard_map/all_to_all | solution.py:246
  101.6 6.0 %collective-permute-start.3 = (bf16[64,24,128]{2,1,0:T(8,128)(2,1)S(1)}, bf16[64,24,128]{2,1,0:T(8,128)(2,1)S(1)}, u32[]{:S(2)}, u32[]{:S(2)}) collective-permute-start(bf16[64,24,128]{2,1,0:T(8,128)(2,1)S(1)} %all_to_all.27.near_ref.got_ref), channel_id=1, source_target_pairs={{0,4},{4,0},{1,5},{5,1},{2,6},{6,2},{3,7},{7,3},{8,12},{12,8},{9,1... | collective-permute-start | bytes 1179656 | tf_op jit(solution)/shard_map/ppermute | solution.py:247
  107.6 0.7 shard_map.174
  108.2 3.3 %all-to-all-start.4 = ((f32[8,8,128]{2,1,0:T(8,128)}), f32[8,8,128]{2,1,0:T(8,128)S(1)}, u32[]{:S(2)}, u32[]{:S(2)}) async-start(f32[8,8,128]{2,1,0:T(8,128)} %shard_map.174), calls=%async_computation.4 | async-start | bytes 65536 | tf_op jit(solution)/shard_map/all_to_all | solution.py:258
  111.8 0.9 shard_map.178
  112.7 0.2 shard_map.176.delta_ref
  112.9 3.5 %all-to-all-done.4.squares_ref = f32[8,8,128]{2,1,0:T(8,128)S(1)} async-done(((f32[8,8,128]{2,1,0:T(8,128)}), f32[8,8,128]{2,1,0:T(8,128)S(1)}, u32[]{:S(2)}, u32[]{:S(2)}) %all-to-all-start.4) | async-done | bytes 32800 | tf_op jit(solution)/shard_map/all_to_all | solution.py:258
  116.4 0.8 shard_map.177
  (24 shorter events, 0.3 us)
Async XLA Ops:
  0.6 40.2 %copy-start.8 = (bf16[16,128]{1,0:T(8,128)(2,1)S(1)}, bf16[16,128]{1,0:T(8,128)(2,1)}, u32[]{:S(2)}) copy-start(bf16[16,128]{1,0:T(8,128)(2,1)} %own_ref.2) | copy-start | bytes 12292
  0.7 34.7 %collective-permute-start.1 = (bf16[768,512]{1,0:T(8,128)(2,1)}, bf16[768,512]{1,0:T(8,128)(2,1)}, u32[]{:S(2)}, u32[]{:S(2)}) collective-permute-start(bf16[768,512]{1,0:T(8,128)(2,1)} %own_ref.3), channel_id=1, source_target_pairs={{0,4},{4,0},{1,5},{5,1},{2,6},{6,2},{3,7},{7,3},{8,12},{12,8},{9,1... | collective-permute-start | bytes 2359304 | tf_op jit(solution)/shard_map/ppermute | solution.py:211
  10.8 24.6 %all-to-all-start = ((bf16[64,16,128]{2,1,0:T(8,128)(2,1)}), bf16[64,16,128]{2,1,0:T(8,128)(2,1)S(1)}, u32[]{:S(2)}, u32[]{:S(2)}) async-start(bf16[64,16,128]{2,1,0:T(8,128)(2,1)} %broadcast_in_dim.3), calls=%async_computation | async-start | bytes 524288 | tf_op jit(solution)/shard_map/all_to_all | solution.py:200
  21.8 1.9 %copy-start = (bf16[768,2048]{1,0:T(8,128)(2,1)S(1)}, bf16[768,2048]{1,0:T(8,128)(2,1)}, u32[]{:S(2)}) copy-start(bf16[768,2048]{1,0:T(8,128)(2,1)} %x_ref.3) | copy-start | bytes 9437188
  23.7 0.7 copy-start.7
  24.4 16.4 %copy-start.1 = (bf16[768,2048]{1,0:T(8,128)(2,1)S(1)}, bf16[768,2048]{1,0:T(8,128)(2,1)}, u32[]{:S(2)}) copy-start(bf16[768,2048]{1,0:T(8,128)(2,1)} %x_ref.3) | copy-start | bytes 9437188
  25.1 3.4 %collective-permute-start = (bf16[64,8,128]{2,1,0:T(8,128)(2,1)S(1)}, bf16[64,8,128]{2,1,0:T(8,128)(2,1)S(1)}, u32[]{:S(2)}, u32[]{:S(2)}) collective-permute-start(bf16[64,8,128]{2,1,0:T(8,128)(2,1)S(1)} %shard_map.169.own_ref), channel_id=1, source_target_pairs={{0,4},{4,0},{1,5},{5,1},{2,6},{6,2},{3,7},{7,3},{8,12},{12,8},{9,1... | collective-permute-start | bytes 393224 | tf_op jit(solution)/shard_map/ppermute | solution.py:213
  35.4 24.6 %copy-start.2 = (bf16[768,512]{1,0:T(8,128)(2,1)S(1)}, bf16[768,512]{1,0:T(8,128)(2,1)}, u32[]{:S(2)}) copy-start(bf16[768,512]{1,0:T(8,128)(2,1)} %own_ref.3) | copy-start | bytes 2359300
  35.4 5.4 %collective-permute-start.2 = (bf16[64,16,128]{2,1,0:T(8,128)(2,1)S(1)}, bf16[64,16,128]{2,1,0:T(8,128)(2,1)S(1)}, u32[]{:S(2)}, u32[]{:S(2)}) collective-permute-start(bf16[64,16,128]{2,1,0:T(8,128)(2,1)S(1)} %all-to-all-done.near_ref), channel_id=1, source_target_pairs={{0,4},{4,0},{1,5},{5,1},{2,6},{6,2},{3,7},{7,3},{8,12},{12,8},{9,1... | collective-permute-start | bytes 786440 | tf_op jit(solution)/shard_map/ppermute | solution.py:216
  42.1 39.0 %copy-start.9 = (f32[4,512]{1,0:T(4,128)S(1)}, f32[4,512]{1,0:T(4,128)}, u32[]{:S(2)}) copy-start(f32[4,512]{1,0:T(4,128)} %mean_ref.1) | copy-start | bytes 24580
  42.1 39.0 %copy-start.10 = (f32[4,512]{1,0:T(4,128)S(1)}, f32[4,512]{1,0:T(4,128)}, u32[]{:S(2)}) copy-start(f32[4,512]{1,0:T(4,128)} %var_ref.1) | copy-start | bytes 24580
  59.9 51.8 %copy-start.3 = (f32[2048,16]{0,1:T(8,128)S(1)}, f32[2048,16]{0,1:T(8,128)}, u32[]{:S(2)}) copy-start(f32[2048,16]{0,1:T(8,128)} %param.17) | copy-start | bytes 393220
  59.9 51.8 %copy-start.4 = (f32[2048,16]{0,1:T(8,128)S(1)}, f32[2048,16]{0,1:T(8,128)}, u32[]{:S(2)}) copy-start(f32[2048,16]{0,1:T(8,128)} %param.18) | copy-start | bytes 393220
  59.9 51.8 %copy-start.5 = (f32[2048,16]{0,1:T(8,128)S(1)}, f32[2048,16]{0,1:T(8,128)}, u32[]{:S(2)}) copy-start(f32[2048,16]{0,1:T(8,128)} %param.19) | copy-start | bytes 393220
  61.8 54.6 %copy-start.6 = (f32[16,512]{1,0:T(8,128)S(1)}, f32[16,512]{1,0:T(8,128)}, u32[]{:S(2)}) copy-start(f32[16,512]{1,0:T(8,128)} %weight_ref.1) | copy-start | bytes 98308
  101.6 11.2 %collective-permute-start.3 = (bf16[64,24,128]{2,1,0:T(8,128)(2,1)S(1)}, bf16[64,24,128]{2,1,0:T(8,128)(2,1)S(1)}, u32[]{:S(2)}, u32[]{:S(2)}) collective-permute-start(bf16[64,24,128]{2,1,0:T(8,128)(2,1)S(1)} %all_to_all.27.near_ref.got_ref), channel_id=1, source_target_pairs={{0,4},{4,0},{1,5},{5,1},{2,6},{6,2},{3,7},{7,3},{8,12},{12,8},{9,1... | collective-permute-start | bytes 1179656 | tf_op jit(solution)/shard_map/ppermute | solution.py:247
  108.2 8.2 %all-to-all-start.4 = ((f32[8,8,128]{2,1,0:T(8,128)}), f32[8,8,128]{2,1,0:T(8,128)S(1)}, u32[]{:S(2)}, u32[]{:S(2)}) async-start(f32[8,8,128]{2,1,0:T(8,128)} %shard_map.174), calls=%async_computation.4 | async-start | bytes 65536 | tf_op jit(solution)/shard_map/all_to_all | solution.py:258

commit v4 on v2

v4 whole, which is shorter than its diff:
```python
import functools

import jax
import jax.numpy as jnp
from jax import lax
from jax.experimental import pallas as pl
from jax.experimental.pallas import tpu as pltpu
from jax.sharding import Mesh
from jax.sharding import PartitionSpec as P

D = 2048
W = 2048
R = 512
H = 16
FS = ("z", "y", "c")
PLANE = ("z", "y")
CHIPS = 64
CHUNK = 20
ROWS = CHIPS * CHUNK
SWAP = [(0, 1), (1, 0)]
BF = jnp.bfloat16
F32 = jnp.float32
VMEM = pl.BlockSpec(memory_space=pltpu.VMEM)


def call(body, outs, count, flops, moved, scratch=()):
    return pl.pallas_call(
        body,
        out_shape=outs,
        in_specs=[VMEM] * count,
        out_specs=jax.tree.map(lambda _: VMEM, outs),
        scratch_shapes=list(scratch),
        compiler_params=pltpu.CompilerParams(vmem_limit_bytes=12 << 20),
        cost_estimate=pl.CostEstimate(flops=flops, bytes_accessed=moved, transcendentals=0),
    )


def shape(dims, dtype):
    return jax.ShapeDtypeStruct(dims, dtype)


def decay_body(cot_ref, x_ref, out_ref):
    part = jnp.dot(cot_ref[...], x_ref[...], preferred_element_type=F32)
    high = part.astype(BF).astype(F32)
    low = part - high
    for b in range(D // 128):
        half, k = (b % 4) // 2, b % 2
        at = (b // 4) * 4 + k
        lanes = slice(b * 128, (b + 1) * 128)
        out_ref[half, pl.ds(at, H, stride=16), :] = high[:, lanes]
        out_ref[half, pl.ds(at + 2, H, stride=16), :] = low[:, lanes]


def project_body(x_ref, near_ref, far_ref, own_ref, out_ref, whole):
    core = lax.axis_index("c")
    whole[:, pl.ds(core, 1)] = near_ref[...].reshape(CHIPS, 1, 16, 128)
    whole[:, pl.ds(1 - core, 1)] = far_ref[...].reshape(CHIPS, 1, 16, 128)
    part = jnp.dot(
        x_ref[...], whole[...].reshape(D, 128), preferred_element_type=F32
    ).astype(BF)
    a = lax.broadcasted_iota(jnp.int32, (128, 128), 0)
    lane = lax.broadcasted_iota(jnp.int32, (128, 128), 1)
    half = jnp.where(a < 64, 1 - core, core)
    source = (a & 15) * 8 + half * 4 + ((a >> 4) & 3)
    order = jnp.where(lane == source, 1.0, 0.0).astype(BF)
    turned = lax.dot_general(
        order, part, (((1,), (1,)), ((), ())), preferred_element_type=F32
    ).astype(BF)
    out_ref[0:128, :] = turned
    out_ref[128:136, :] = jnp.zeros((8, 768), BF)
    out_ref[128:136, 0:128] = own_ref[0:8]
    out_ref[128:136, 128:256] = own_ref[8:16]


def gradient_body(half, p_ref, v_ref, dec_ref, out_ref, rows):
    core = lax.axis_index("c")
    for q in range(4):
        part = jnp.dot(
            p_ref[q, half * 64 : half * 64 + 64, :], v_ref[...], preferred_element_type=F32
        )
        for i in range(4):
            for cb in range(4):
                rows[pl.ds(q * 16 * CHUNK + cb * 4 + i, 16, stride=CHUNK), :] = part[
                    i * 16 : i * 16 + 16, cb * 128 : cb * 128 + 128
                ]
    side = core if half == 1 else 1 - core
    for k in range(4):
        rows[pl.ds(16 + k, CHIPS, stride=CHUNK), :] = dec_ref[
            side, pl.ds(k, CHIPS, stride=4), :
        ]
    out_ref[...] = rows[...].astype(BF)


def pair_body(own_ref, peer_ref, out_ref, rows):
    rows[...] = own_ref[...].astype(F32) + peer_ref[...].astype(F32)
    for k in range(2):
        at = pl.ds(16 + k, CHIPS, stride=CHUNK)
        below = pl.ds(18 + k, CHIPS, stride=CHUNK)
        total = rows[at, :] + rows[below, :]
        high = total.astype(BF).astype(F32)
        rows[at, :] = high
        rows[below, :] = total - high
    out_ref[...] = rows[...].astype(BF)


def moment_body(got_ref, mean_ref, var_ref, out_ref, mean_out, var_out, mean_s, var_s, sums, new):
    for cb in range(4):
        lanes = slice(cb * 128, cb * 128 + 128)
        mean_s[cb * 4 : cb * 4 + 4, :] = mean_ref[:, lanes]
        var_s[cb * 4 : cb * 4 + 4, :] = var_ref[:, lanes]
    sums[...] = jnp.sum(got_ref[...].astype(F32).reshape(CHIPS // 2, 2 * CHUNK, 128), axis=0)
    grad = sums[0:16, :] + sums[CHUNK : CHUNK + 16, :]
    dec = (
        sums[16:18, :]
        + sums[18:20, :]
        + sums[CHUNK + 16 : CHUNK + 18, :]
        + sums[CHUNK + 18 : CHUNK + 20, :]
    )
    mean_new = 0.9 * mean_s[...] + 0.1 * grad
    var_new = 0.95 * var_s[...] + 0.05 * grad * grad
    ratio = mean_new / (jnp.sqrt(var_new) + 1e-08)
    mean_s[...] = mean_new
    var_s[...] = var_new
    for cb in range(4):
        lanes = slice(cb * 128, cb * 128 + 128)
        mean_out[:, lanes] = mean_s[cb * 4 : cb * 4 + 4, :]
        var_out[:, lanes] = var_s[cb * 4 : cb * 4 + 4, :]
    high = dec.astype(BF).astype(F32)
    for copy in range(4):
        new[copy * CHUNK : copy * CHUNK + 16, :] = ratio
        new[copy * CHUNK + 16 : copy * CHUNK + 18, :] = high
        new[copy * CHUNK + 18 : copy * CHUNK + 20, :] = dec - high
    four = new[...].astype(BF)
    for at in range(0, ROWS, 4 * CHUNK):
        out_ref[at : at + 4 * CHUNK, :] = four


def spread_body(p_ref, out_ref):
    core = lax.axis_index("c")
    wide = 16 * CHUNK
    lane = lax.broadcasted_iota(jnp.int32, (128, wide), 0)
    k = lax.broadcasted_iota(jnp.int32, (128, wide), 1)
    chip = (k * 3277) >> 16
    row = k - chip * CHUNK
    mine = lax.broadcasted_iota(jnp.int32, (16, wide), 1)
    column = (mine - ((mine * 3277) >> 16) * CHUNK) >> 2
    for side in range(2):
        half = core if side == 0 else 1 - core
        hit = (lane == chip * 8 + half * 4 + (row & 3)) & (row < 16)
        pick = jnp.where(hit, 1.0, 0.0).astype(BF)
        for q in range(4):
            own = jnp.concatenate(
                [
                    p_ref[q, 128:136, 0:128].astype(F32),
                    p_ref[q, 128:136, 128:256].astype(F32),
                ]
            ).astype(BF)
            rows = jnp.dot(own, pick, preferred_element_type=F32)
            for cb in range(4):
                out_ref[side, q, cb * 16 : cb * 16 + 16, :] = jnp.where(
                    column == cb, rows, 0.0
                ).astype(BF)


def decay_update_body(
    near_ref, far_ref, weight_ref, mean_ref, var_ref, new_out, copy_out, mean_out, var_out, rows
):
    core = lax.axis_index("c")
    rows[core] = near_ref[...].astype(F32)
    rows[1 - core] = far_ref[...].astype(F32)
    for b in range(D // 128):
        half, k = (b % 4) // 2, b % 2
        at = (b // 4) * CHUNK + 16 + k
        lanes = slice(b * 128, (b + 1) * 128)
        grad = (
            rows[half, pl.ds(at, H, stride=4 * CHUNK), :]
            + rows[half, pl.ds(at + 2, H, stride=4 * CHUNK), :]
        )
        mean_new = 0.9 * mean_ref[:, lanes] + 0.1 * grad
        var_new = 0.95 * var_ref[:, lanes] + 0.05 * grad * grad
        new = weight_ref[:, lanes] - 0.5 * mean_new / (jnp.sqrt(var_new) + 1e-08)
        mean_out[:, lanes] = mean_new
        var_out[:, lanes] = var_new
        new_out[:, lanes] = new
        copy_out[:, lanes] = new.astype(BF)


def squares_body(near_ref, out_ref):
    near = near_ref[...].astype(F32).reshape(CHIPS // 4, 4 * CHUNK, 128)
    row = lax.broadcasted_iota(jnp.int32, (4 * CHUNK, 128), 0)
    row = row - ((row * 3277) >> 16) * CHUNK
    sums = jnp.where(row < 16, jnp.sum(near * near, axis=0), 0.0)
    sums = jnp.sum(sums.reshape(CHUNK // 2, 8, 128), axis=0)
    out_ref[...] = jnp.broadcast_to(sums[None], (8, 8, 128))


def product_body(rows_ref, near_ref, far_ref, out_ref):
    got = jnp.zeros((64, 128), F32)
    for q in range(4):
        part = slice(q * 16 * CHUNK, (q + 1) * 16 * CHUNK)
        got += jnp.dot(rows_ref[0, q], near_ref[part, :], preferred_element_type=F32)
        got += jnp.dot(rows_ref[1, q], far_ref[part, :], preferred_element_type=F32)
    for cb in range(4):
        out_ref[:, cb * 128 : cb * 128 + 128] = got[cb * 16 : cb * 16 + 16]


def step_body(squares_ref, delta_ref, weight_ref, step_out, new_out, copy_out):
    root_mean = jnp.sqrt(jnp.sum(squares_ref[...]) / (R * W) + 1e-06)
    step = -0.5 / root_mean * delta_ref[...]
    new = weight_ref[...] + step
    step_out[...] = step
    new_out[...] = new
    copy_out[...] = new.astype(BF)


def local(
    inputs,
    values_cot,
    decay_cot,
    factor,
    value_weight,
    lowrank_mean,
    lowrank_var,
    decay_weight,
    decay_mean,
    decay_var,
):
    chunk = shape((ROWS, 128), BF)

    def across(rows):
        tiles = rows.reshape(CHIPS, CHUNK // 4, 4, 128)
        return lax.all_to_all(tiles, PLANE, 0, 0, tiled=True).reshape(ROWS, 128)

    near = lax.all_to_all(
        jnp.broadcast_to(factor, (CHIPS, 16, 128)), PLANE, 0, 0, tiled=True
    )
    decay_rows = call(
        decay_body,
        shape((2, CHIPS * 4, 128), F32),
        2,
        2 * 768 * D * H,
        4 << 20,
    )(decay_cot.T, inputs)
    near, decay_rows = lax.optimization_barrier((near, decay_rows))
    far = lax.ppermute(near, "c", SWAP)
    quarter = call(
        project_body,
        shape((136, 768), BF),
        4,
        2 * 768 * D * 128,
        4 << 20,
        [pltpu.VMEM((CHIPS, 2, 16, 128), BF)],
    )(inputs, near, far, factor)
    projected = lax.all_gather(quarter, "x")

    def gradient(half):
        return call(
            functools.partial(gradient_body, half),
            chunk,
            3,
            2 * 768 * 256 * 512,
            2 << 20,
            [pltpu.VMEM((ROWS, 128), F32)],
        )(projected, values_cot, decay_rows)

    peer = lax.ppermute(gradient(0), "c", SWAP)
    paired = call(
        pair_body, chunk, 2, 400000, 1 << 20, [pltpu.VMEM((ROWS, 128), F32)]
    )(gradient(1), peer)
    arrived = across(paired)
    rows = call(spread_body, shape((2, 4, 64, 16 * CHUNK), BF), 1, 8 * 2 * 16 * 128 * 256, 1 << 20)(
        projected
    )
    ratio, mean_new, var_new = call(
        moment_body,
        (chunk, shape((4, 512), F32), shape((4, 512), F32)),
        3,
        400000,
        1 << 20,
        [
            pltpu.VMEM((16, 128), F32),
            pltpu.VMEM((16, 128), F32),
            pltpu.VMEM((2 * CHUNK, 128), F32),
            pltpu.VMEM((4 * CHUNK, 128), F32),
        ],
    )(arrived, lowrank_mean, lowrank_var)
    near = across(ratio)
    far = lax.ppermute(near, "c", SWAP)
    state = shape((H, D), F32)
    decay_new, decay_copy, decay_mean_new, decay_var_new = call(
        decay_update_body,
        (state, shape((H, D), BF), state, state),
        5,
        400000,
        1 << 20,
        [pltpu.VMEM((2, ROWS, 128), F32)],
    )(near, far, decay_weight.T, decay_mean.T, decay_var.T)
    squares = call(squares_body, shape((8, 8, 128), F32), 1, 400000, 1 << 20)(near)
    squares = lax.all_to_all(squares, ("c", "x"), 0, 0, tiled=True)
    delta = call(
        product_body, shape((16, 512), F32), 3, 2 * 64 * 2048 * 128, 1 << 20
    )(rows, near, far)
    block = shape((16, 512), F32)
    value_step, value_new, value_copy = call(
        step_body, (block, block, shape((16, 512), BF)), 3, 40000, 100000
    )(squares, delta, value_weight)
    return (
        value_step,
        value_new,
        value_copy,
        mean_new,
        var_new,
        decay_new.T,
        decay_copy.T,
        decay_mean_new.T,
        decay_var_new.T,
    )


def solution(mesh):
    split = Mesh(mesh.devices.reshape(8, 8, 2, mesh.shape["tp"]), ("z", "y", "c", "x"))
    placed = (
        P(FS, None),
        P(FS, "x"),
        P(FS, None),
        P(FS, "x"),
        P(FS, "x"),
        P(FS, "x"),
        P(FS, "x"),
        P(),
        P(),
        P(),
    )
    return jax.shard_map(
        local,
        mesh=split,
        in_specs=placed,
        out_specs=(P(FS, "x"),) * 5 + (P(),) * 4,
        check_vma=False,
    )
```

time: 116 us -> 115 us (level)
  blocking collectives: 51.6 us -> 49.2 us
    all_to_all x2, blocking collectives: 39.2 us -> 37 us  [across(): return lax.all_to_all(tiles, PLANE, 0, 0, tiled=True).reshape(ROWS, 128)]
  transfers between devices with their start and end apart: 5 -> 5, of which waited for: 4 -> 4; matrix products, arithmetic and copies ran while one was open for 0% -> 0% of each run, Pallas kernels for 3% -> 2%
where the time goes in v4:
time: 115 us; the launch traced here: 114 us
  blocking collectives  49.2 us (43%)
  starting transfers between devices  36.7 us (32%)
  waiting for transfers between devices  15.7 us (14%)
  Pallas kernels  7.92 us (7%)
  local copies, waits for them, and re-layouts  4.14 us (4%)
    all_to_all x2, blocking collectives, across(): return lax.all_to_all(tiles, PLANE, 0, 0, tiled=True).reshape(ROWS, 128)  37 us
    all_to_all x1, starting transfers between devices, local(): lax.all_to_all(jnp.broadcast_to(factor, (CHIPS, 16, 128)), PLANE, 0, 0, t...  17.4 us
    all_gather x1, blocking collectives, local(): projected = lax.all_gather(quarter, 'x')  12.2 us
    ppermute x2, starting transfers between devices, local(): far = lax.ppermute(near, 'c', SWAP)  10.7 us
    all_to_all x1, waiting for transfers between devices, local(): lax.all_to_all(jnp.broadcast_to(factor, (CHIPS, 16, 128)), PLANE, 0, 0, t...  9.47 us
    all_to_all x1, starting transfers between devices, local(): squares = lax.all_to_all(squares, ('c', 'x'), 0, 0, tiled=True)  4.55 us
    all_to_all x1, waiting for transfers between devices, local(): squares = lax.all_to_all(squares, ('c', 'x'), 0, 0, tiled=True)  4.37 us
    ppermute x1, starting transfers between devices, local(): peer = lax.ppermute(gradient(0), 'c', SWAP)  4.12 us
  transfers between devices with their start and end apart: 5, of which 4 were waited for; matrix products, arithmetic and copies ran while one was open for 0% of the time, Pallas kernels for 2%

profile of v4, /device:TPU:1, one launch (start us, length us, event | category | flops | bytes accessed | tf_op | source)
XLA Modules:
  0.0 114.5 jit_solution(4458814860773268482)
XLA Ops:
  0.7 1.5 %broadcast_in_dim.3 = bf16[64,16,128]{2,1,0:T(8,128)(2,1)} broadcast(bf16[16,128]{1,0:T(8,128)(2,1)} %own_ref.1), dimensions={1,2} | broadcast | bytes 266240 | tf_op jit(solution)/shard_map/broadcast_in_dim | solution.py:235
  2.1 17.4 %all-to-all-start = ((bf16[64,16,128]{2,1,0:T(8,128)(2,1)}), bf16[64,16,128]{2,1,0:T(8,128)(2,1)}, u32[]{:S(2)}, u32[]{:S(2)}) async-start(bf16[64,16,128]{2,1,0:T(8,128)(2,1)} %broadcast_in_dim.3), calls=%async_computation | async-start | bytes 524288 | tf_op jit(solution)/shard_map/all_to_all | solution.py:234
  19.5 1.9 %copy-done = bf16[768,2048]{1,0:T(8,128)(2,1)S(1)} copy-done((bf16[768,2048]{1,0:T(8,128)(2,1)S(1)}, bf16[768,2048]{1,0:T(8,128)(2,1)}, u32[]{:S(2)}) %copy-start) | copy-done | bytes 3145752
  21.4 0.7 copy-done.7
  22.2 0.6 shard_map.169.dec_ref
  22.7 9.5 %all-to-all-done.near_ref = bf16[64,16,128]{2,1,0:T(8,128)(2,1)} async-done(((bf16[64,16,128]{2,1,0:T(8,128)(2,1)}), bf16[64,16,128]{2,1,0:T(8,128)(2,1)}, u32[]{:S(2)}, u32[]{:S(2)}) %all-to-all-start) | async-done | bytes 262176 | tf_op jit(solution)/shard_map/all_to_all | solution.py:234
  32.2 5.1 %collective-permute-start = (bf16[64,16,128]{2,1,0:T(8,128)(2,1)}, bf16[64,16,128]{2,1,0:T(8,128)(2,1)S(1)}, u32[]{:S(2)}, u32[]{:S(2)}) collective-permute-start(bf16[64,16,128]{2,1,0:T(8,128)(2,1)} %all-to-all-done.near_ref), channel_id=1, source_target_pairs={{0,4},{4,0},{1,5},{5,1},{2,6},{6,2},{3,7},{7,3},{8,12},{12,8},{9,1... | collective-permute-start | bytes 786440 | tf_op jit(solution)/shard_map/ppermute | solution.py:245
  37.3 1.4 %collective-permute-done.far_ref = bf16[64,16,128]{2,1,0:T(8,128)(2,1)S(1)} collective-permute-done((bf16[64,16,128]{2,1,0:T(8,128)(2,1)}, bf16[64,16,128]{2,1,0:T(8,128)(2,1)S(1)}, u32[]{:S(2)}, u32[]{:S(2)}) %collective-permute-start) | collective-permute-done | bytes 262176 | tf_op jit(solution)/shard_map/ppermute | solution.py:245
  38.7 2.2 %shard_map.170 = bf16[136,768]{1,0:T(8,128)(2,1)S(1)} custom-call(bf16[768,2048]{1,0:T(8,128)(2,1)S(1)} %copy-done.1, bf16[64,16,128]{2,1,0:T(8,128)(2,1)} %all-to-all-done.near_ref, bf16[64,16,128]{2,1,0:T(8,128)(2,1)S(1)} %collective-permute-done.far_ref, bf16[16,128]{1,0:T(8,128)(2,1)S(1)} %copy-done.8), custom_call_target="tpu_custom_call" | custom-call | flops 402653184 | bytes 4194304 | tf_op jit(solution)/shard_map/pallas_call | solution.py:246
  40.9 12.2 %all-gather = bf16[544,768]{1,0:T(8,128)(2,1)S(1)} all-gather(bf16[136,768]{1,0:T(8,128)(2,1)S(1)} %shard_map.170), channel_id=2, replica_groups=mesh['z'=8,'y'=8,'c'=2,'x'=4] {'x'}, dimensions={0}, use_global_device_ids=true | all-gather | bytes 1044480 | tf_op jit(solution)/shard_map/all_gather | solution.py:254
  53.1 0.7 shard_map.172
  53.7 4.1 %collective-permute-start.1 = (bf16[1280,128]{1,0:T(8,128)(2,1)S(1)}, bf16[1280,128]{1,0:T(8,128)(2,1)S(1)}, u32[]{:S(2)}, u32[]{:S(2)}) collective-permute-start(bf16[1280,128]{1,0:T(8,128)(2,1)S(1)} %shard_map.172), channel_id=1, source_target_pairs={{0,4},{4,0},{1,5},{5,1},{2,6},{6,2},{3,7},{7,3},{8,12},{12,8},{9,1... | collective-permute-start | bytes 983048 | tf_op jit(solution)/shard_map/ppermute | solution.py:266
  57.9 0.7 shard_map.171.own_ref
  58.6 0.5 collective-permute-done.1.peer_ref
  59.3 18.2 %all_to_all.20 = bf16[64,5,4,128]{3,2,1,0:T(4,128)(2,1)S(1)} all-to-all(bf16[64,5,4,128]{3,2,1,0:T(4,128)(2,1)S(1)} %bitcast.21), channel_id=1, replica_groups=mesh['z'=8,'y'=8,'c'=2,'x'=4] {'z','y'}, dimensions={0} | all-to-all | bytes 655360 | tf_op jit(solution)/shard_map/all_to_all | solution.py:232
  77.4 0.7 shard_map.174
  78.1 18.8 %all_to_all.21 = bf16[64,5,4,128]{3,2,1,0:T(4,128)(2,1)S(1)} all-to-all(bf16[64,5,4,128]{3,2,1,0:T(4,128)(2,1)S(1)} %bitcast.22), channel_id=1, replica_groups=mesh['z'=8,'y'=8,'c'=2,'x'=4] {'z','y'}, dimensions={0} | all-to-all | bytes 655360 | tf_op jit(solution)/shard_map/all_to_all | solution.py:232
  96.9 5.6 %collective-permute-start.2 = (bf16[1280,128]{1,0:T(8,128)(2,1)S(1)}, bf16[1280,128]{1,0:T(8,128)(2,1)S(1)}, u32[]{:S(2)}, u32[]{:S(2)}) collective-permute-start(bf16[1280,128]{1,0:T(8,128)(2,1)S(1)} %bitcast.16), channel_id=1, source_target_pairs={{0,4},{4,0},{1,5},{5,1},{2,6},{6,2},{3,7},{7,3},{8,12},{12,8},{9,1... | collective-permute-start | bytes 983048 | tf_op jit(solution)/shard_map/ppermute | solution.py:288
  102.5 0.7 shard_map.175
  103.2 4.6 %all-to-all-start.3 = ((f32[8,8,128]{2,1,0:T(8,128)}), f32[8,8,128]{2,1,0:T(8,128)S(1)}, u32[]{:S(2)}, u32[]{:S(2)}) async-start(f32[8,8,128]{2,1,0:T(8,128)} %shard_map.175), calls=%async_computation.3 | async-start | bytes 65536 | tf_op jit(solution)/shard_map/all_to_all | solution.py:299
  107.7 0.3 shard_map.176.rows_ref
  108.3 4.4 %all-to-all-done.3.squares_ref = f32[8,8,128]{2,1,0:T(8,128)S(1)} async-done(((f32[8,8,128]{2,1,0:T(8,128)}), f32[8,8,128]{2,1,0:T(8,128)S(1)}, u32[]{:S(2)}, u32[]{:S(2)}) %all-to-all-start.3) | async-done | bytes 32800 | tf_op jit(solution)/shard_map/all_to_all | solution.py:299
  112.6 0.8 shard_map.178
  113.5 1.0 shard_map.179
  (23 shorter events, 0.5 us)
Async XLA Ops:
  0.6 38.0 %copy-start.8 = (bf16[16,128]{1,0:T(8,128)(2,1)S(1)}, bf16[16,128]{1,0:T(8,128)(2,1)}, u32[]{:S(2)}) copy-start(bf16[16,128]{1,0:T(8,128)(2,1)} %own_ref.1) | copy-start | bytes 12292
  2.1 30.1 %all-to-all-start = ((bf16[64,16,128]{2,1,0:T(8,128)(2,1)}), bf16[64,16,128]{2,1,0:T(8,128)(2,1)}, u32[]{:S(2)}, u32[]{:S(2)}) async-start(bf16[64,16,128]{2,1,0:T(8,128)(2,1)} %broadcast_in_dim.3), calls=%async_computation | async-start | bytes 524288 | tf_op jit(solution)/shard_map/all_to_all | solution.py:234
  19.5 1.9 %copy-start = (bf16[768,2048]{1,0:T(8,128)(2,1)S(1)}, bf16[768,2048]{1,0:T(8,128)(2,1)}, u32[]{:S(2)}) copy-start(bf16[768,2048]{1,0:T(8,128)(2,1)} %x_ref.3) | copy-start | bytes 9437188
  21.4 0.7 copy-start.7
  22.2 16.5 %copy-start.1 = (bf16[768,2048]{1,0:T(8,128)(2,1)S(1)}, bf16[768,2048]{1,0:T(8,128)(2,1)}, u32[]{:S(2)}) copy-start(bf16[768,2048]{1,0:T(8,128)(2,1)} %x_ref.3) | copy-start | bytes 9437188
  32.2 20.9 %copy-start.2 = (bf16[768,512]{1,0:T(8,128)(2,1)S(1)}, bf16[768,512]{1,0:T(8,128)(2,1)}, u32[]{:S(2)}) copy-start(bf16[768,512]{1,0:T(8,128)(2,1)} %v_ref.3) | copy-start | bytes 2359300
  32.2 6.4 %collective-permute-start = (bf16[64,16,128]{2,1,0:T(8,128)(2,1)}, bf16[64,16,128]{2,1,0:T(8,128)(2,1)S(1)}, u32[]{:S(2)}, u32[]{:S(2)}) collective-permute-start(bf16[64,16,128]{2,1,0:T(8,128)(2,1)} %all-to-all-done.near_ref), channel_id=1, source_target_pairs={{0,4},{4,0},{1,5},{5,1},{2,6},{6,2},{3,7},{7,3},{8,12},{12,8},{9,1... | collective-permute-start | bytes 786440 | tf_op jit(solution)/shard_map/ppermute | solution.py:245
  53.1 24.4 %copy-start.9 = (f32[4,512]{1,0:T(4,128)S(1)}, f32[4,512]{1,0:T(4,128)}, u32[]{:S(2)}) copy-start(f32[4,512]{1,0:T(4,128)} %mean_ref.1) | copy-start | bytes 24580
  53.1 24.4 %copy-start.10 = (f32[4,512]{1,0:T(4,128)S(1)}, f32[4,512]{1,0:T(4,128)}, u32[]{:S(2)}) copy-start(f32[4,512]{1,0:T(4,128)} %var_ref.1) | copy-start | bytes 24580
  53.7 5.4 %collective-permute-start.1 = (bf16[1280,128]{1,0:T(8,128)(2,1)S(1)}, bf16[1280,128]{1,0:T(8,128)(2,1)S(1)}, u32[]{:S(2)}, u32[]{:S(2)}) collective-permute-start(bf16[1280,128]{1,0:T(8,128)(2,1)S(1)} %shard_map.172), channel_id=1, source_target_pairs={{0,4},{4,0},{1,5},{5,1},{2,6},{6,2},{3,7},{7,3},{8,12},{12,8},{9,1... | collective-permute-start | bytes 983048 | tf_op jit(solution)/shard_map/ppermute | solution.py:266
  58.6 54.1 %copy-start.6 = (f32[16,512]{1,0:T(8,128)S(1)}, f32[16,512]{1,0:T(8,128)}, u32[]{:S(2)}) copy-start(f32[16,512]{1,0:T(8,128)} %weight_ref.1) | copy-start | bytes 98308
  58.6 54.9 %copy-start.3 = (f32[2048,16]{0,1:T(8,128)S(1)}, f32[2048,16]{0,1:T(8,128)}, u32[]{:S(2)}) copy-start(f32[2048,16]{0,1:T(8,128)} %param.17) | copy-start | bytes 393220
  58.6 54.9 %copy-start.4 = (f32[2048,16]{0,1:T(8,128)S(1)}, f32[2048,16]{0,1:T(8,128)}, u32[]{:S(2)}) copy-start(f32[2048,16]{0,1:T(8,128)} %param.18) | copy-start | bytes 393220
  58.6 54.9 %copy-start.5 = (f32[2048,16]{0,1:T(8,128)S(1)}, f32[2048,16]{0,1:T(8,128)}, u32[]{:S(2)}) copy-start(f32[2048,16]{0,1:T(8,128)} %param.19) | copy-start | bytes 393220
  96.9 11.1 %collective-permute-start.2 = (bf16[1280,128]{1,0:T(8,128)(2,1)S(1)}, bf16[1280,128]{1,0:T(8,128)(2,1)S(1)}, u32[]{:S(2)}, u32[]{:S(2)}) collective-permute-start(bf16[1280,128]{1,0:T(8,128)(2,1)S(1)} %bitcast.16), channel_id=1, source_target_pairs={{0,4},{4,0},{1,5},{5,1},{2,6},{6,2},{3,7},{7,3},{8,12},{12,8},{9,1... | collective-permute-start | bytes 983048 | tf_op jit(solution)/shard_map/ppermute | solution.py:288
  103.2 9.5 %all-to-all-start.3 = ((f32[8,8,128]{2,1,0:T(8,128)}), f32[8,8,128]{2,1,0:T(8,128)S(1)}, u32[]{:S(2)}, u32[]{:S(2)}) async-start(f32[8,8,128]{2,1,0:T(8,128)} %shard_map.175), calls=%async_computation.3 | async-start | bytes 65536 | tf_op jit(solution)/shard_map/all_to_all | solution.py:299

commit v5 on v4

--- a/solution.py
+++ b/solution.py
@@ -15,7 +15,7 @@
 FS = ("z", "y", "c")
 PLANE = ("z", "y")
 CHIPS = 64
-CHUNK = 20
+CHUNK = 18
 ROWS = CHIPS * CHUNK
 SWAP = [(0, 1), (1, 0)]
 BF = jnp.bfloat16
@@ -39,16 +39,12 @@
     return jax.ShapeDtypeStruct(dims, dtype)
 
 
-def decay_body(cot_ref, x_ref, out_ref):
+def decay_body(cot_ref, x_ref, out_ref, rows):
     part = jnp.dot(cot_ref[...], x_ref[...], preferred_element_type=F32)
-    high = part.astype(BF).astype(F32)
-    low = part - high
     for b in range(D // 128):
-        half, k = (b % 4) // 2, b % 2
-        at = (b // 4) * 4 + k
-        lanes = slice(b * 128, (b + 1) * 128)
-        out_ref[half, pl.ds(at, H, stride=16), :] = high[:, lanes]
-        out_ref[half, pl.ds(at + 2, H, stride=16), :] = low[:, lanes]
+        half, at = (b % 4) // 2, (b // 4) * 2 + b % 2
+        rows[half, pl.ds(at, H, stride=8), :] = part[:, b * 128 : (b + 1) * 128]
+    out_ref[...] = rows[...].astype(BF)
 
 
 def project_body(x_ref, near_ref, far_ref, own_ref, out_ref, whole):
@@ -67,12 +63,11 @@
         order, part, (((1,), (1,)), ((), ())), preferred_element_type=F32
     ).astype(BF)
     out_ref[0:128, :] = turned
-    out_ref[128:136, :] = jnp.zeros((8, 768), BF)
-    out_ref[128:136, 0:128] = own_ref[0:8]
-    out_ref[128:136, 128:256] = own_ref[8:16]
-
-
-def gradient_body(half, p_ref, v_ref, dec_ref, out_ref, rows):
+    out_ref[128:144, :] = jnp.zeros((16, 768), BF)
+    out_ref[128:144, 0:128] = own_ref[...]
+
+
+def gradient_body(half, p_ref, v_ref, dec_ref, out_ref, rows, dec):
     core = lax.axis_index("c")
     for q in range(4):
         part = jnp.dot(
@@ -84,23 +79,18 @@
                     i * 16 : i * 16 + 16, cb * 128 : cb * 128 + 128
                 ]
     side = core if half == 1 else 1 - core
-    for k in range(4):
-        rows[pl.ds(16 + k, CHIPS, stride=CHUNK), :] = dec_ref[
-            side, pl.ds(k, CHIPS, stride=4), :
-        ]
+    dec[...] = dec_ref[side].astype(F32)
+    for k in range(2):
+        rows[pl.ds(16 + k, CHIPS, stride=CHUNK), :] = dec[pl.ds(k, CHIPS, stride=2), :]
     out_ref[...] = rows[...].astype(BF)
 
 
-def pair_body(own_ref, peer_ref, out_ref, rows):
-    rows[...] = own_ref[...].astype(F32) + peer_ref[...].astype(F32)
-    for k in range(2):
-        at = pl.ds(16 + k, CHIPS, stride=CHUNK)
-        below = pl.ds(18 + k, CHIPS, stride=CHUNK)
-        total = rows[at, :] + rows[below, :]
-        high = total.astype(BF).astype(F32)
-        rows[at, :] = high
-        rows[below, :] = total - high
-    out_ref[...] = rows[...].astype(BF)
+def copies_body(own_ref, out_ref):
+    out_ref[...] = jnp.broadcast_to(own_ref[...][None], (CHIPS, 16, 128))
+
+
+def pair_body(own_ref, peer_ref, out_ref):
+    out_ref[...] = (own_ref[...].astype(F32) + peer_ref[...].astype(F32)).astype(BF)
 
 
 def moment_body(got_ref, mean_ref, var_ref, out_ref, mean_out, var_out, mean_s, var_s, sums, new):
@@ -108,14 +98,14 @@
         lanes = slice(cb * 128, cb * 128 + 128)
         mean_s[cb * 4 : cb * 4 + 4, :] = mean_ref[:, lanes]
         var_s[cb * 4 : cb * 4 + 4, :] = var_ref[:, lanes]
-    sums[...] = jnp.sum(got_ref[...].astype(F32).reshape(CHIPS // 2, 2 * CHUNK, 128), axis=0)
-    grad = sums[0:16, :] + sums[CHUNK : CHUNK + 16, :]
-    dec = (
-        sums[16:18, :]
-        + sums[18:20, :]
-        + sums[CHUNK + 16 : CHUNK + 18, :]
-        + sums[CHUNK + 18 : CHUNK + 20, :]
-    )
+    sums[...] = jnp.sum(got_ref[...].astype(F32).reshape(CHIPS // 4, 4 * CHUNK, 128), axis=0)
+    total = (
+        sums[0:CHUNK, :]
+        + sums[CHUNK : 2 * CHUNK, :]
+        + sums[2 * CHUNK : 3 * CHUNK, :]
+        + sums[3 * CHUNK : 4 * CHUNK, :]
+    )
+    grad = total[0:16]
     mean_new = 0.9 * mean_s[...] + 0.1 * grad
     var_new = 0.95 * var_s[...] + 0.05 * grad * grad
     ratio = mean_new / (jnp.sqrt(var_new) + 1e-08)
@@ -125,14 +115,12 @@
         lanes = slice(cb * 128, cb * 128 + 128)
         mean_out[:, lanes] = mean_s[cb * 4 : cb * 4 + 4, :]
         var_out[:, lanes] = var_s[cb * 4 : cb * 4 + 4, :]
-    high = dec.astype(BF).astype(F32)
-    for copy in range(4):
+    for copy in range(8):
         new[copy * CHUNK : copy * CHUNK + 16, :] = ratio
-        new[copy * CHUNK + 16 : copy * CHUNK + 18, :] = high
-        new[copy * CHUNK + 18 : copy * CHUNK + 20, :] = dec - high
-    four = new[...].astype(BF)
-    for at in range(0, ROWS, 4 * CHUNK):
-        out_ref[at : at + 4 * CHUNK, :] = four
+        new[copy * CHUNK + 16 : copy * CHUNK + 18, :] = total[16:18]
+    eight = new[...].astype(BF)
+    for at in range(0, ROWS, 8 * CHUNK):
+        out_ref[at : at + 8 * CHUNK, :] = eight
 
 
 def spread_body(p_ref, out_ref):
@@ -140,22 +128,16 @@
     wide = 16 * CHUNK
     lane = lax.broadcasted_iota(jnp.int32, (128, wide), 0)
     k = lax.broadcasted_iota(jnp.int32, (128, wide), 1)
-    chip = (k * 3277) >> 16
+    chip = (k * 3641) >> 16
     row = k - chip * CHUNK
     mine = lax.broadcasted_iota(jnp.int32, (16, wide), 1)
-    column = (mine - ((mine * 3277) >> 16) * CHUNK) >> 2
+    column = (mine - ((mine * 3641) >> 16) * CHUNK) >> 2
     for side in range(2):
         half = core if side == 0 else 1 - core
         hit = (lane == chip * 8 + half * 4 + (row & 3)) & (row < 16)
         pick = jnp.where(hit, 1.0, 0.0).astype(BF)
         for q in range(4):
-            own = jnp.concatenate(
-                [
-                    p_ref[q, 128:136, 0:128].astype(F32),
-                    p_ref[q, 128:136, 128:256].astype(F32),
-                ]
-            ).astype(BF)
-            rows = jnp.dot(own, pick, preferred_element_type=F32)
+            rows = jnp.dot(p_ref[q, 128:144, 0:128], pick, preferred_element_type=F32)
             for cb in range(4):
                 out_ref[side, q, cb * 16 : cb * 16 + 16, :] = jnp.where(
                     column == cb, rows, 0.0
@@ -172,10 +154,7 @@
         half, k = (b % 4) // 2, b % 2
         at = (b // 4) * CHUNK + 16 + k
         lanes = slice(b * 128, (b + 1) * 128)
-        grad = (
-            rows[half, pl.ds(at, H, stride=4 * CHUNK), :]
-            + rows[half, pl.ds(at + 2, H, stride=4 * CHUNK), :]
-        )
+        grad = rows[half, pl.ds(at, H, stride=4 * CHUNK), :]
         mean_new = 0.9 * mean_ref[:, lanes] + 0.1 * grad
         var_new = 0.95 * var_ref[:, lanes] + 0.05 * grad * grad
         new = weight_ref[:, lanes] - 0.5 * mean_new / (jnp.sqrt(var_new) + 1e-08)
@@ -188,9 +167,9 @@
 def squares_body(near_ref, out_ref):
     near = near_ref[...].astype(F32).reshape(CHIPS // 4, 4 * CHUNK, 128)
     row = lax.broadcasted_iota(jnp.int32, (4 * CHUNK, 128), 0)
-    row = row - ((row * 3277) >> 16) * CHUNK
+    row = row - ((row * 3641) >> 16) * CHUNK
     sums = jnp.where(row < 16, jnp.sum(near * near, axis=0), 0.0)
-    sums = jnp.sum(sums.reshape(CHUNK // 2, 8, 128), axis=0)
+    sums = jnp.sum(sums.reshape(4 * CHUNK // 8, 8, 128), axis=0)
     out_ref[...] = jnp.broadcast_to(sums[None], (8, 8, 128))
 
 
@@ -228,24 +207,24 @@
     chunk = shape((ROWS, 128), BF)
 
     def across(rows):
-        tiles = rows.reshape(CHIPS, CHUNK // 4, 4, 128)
+        tiles = rows.reshape(CHIPS, CHUNK // 2, 2, 128)
         return lax.all_to_all(tiles, PLANE, 0, 0, tiled=True).reshape(ROWS, 128)
 
-    near = lax.all_to_all(
-        jnp.broadcast_to(factor, (CHIPS, 16, 128)), PLANE, 0, 0, tiled=True
-    )
+    copies = call(copies_body, shape((CHIPS, 16, 128), BF), 1, 0, 1 << 18)(factor)
+    near = lax.all_to_all(copies, PLANE, 0, 0, tiled=True)
     decay_rows = call(
         decay_body,
-        shape((2, CHIPS * 4, 128), F32),
+        shape((2, CHIPS * 2, 128), BF),
         2,
         2 * 768 * D * H,
         4 << 20,
+        [pltpu.VMEM((2, CHIPS * 2, 128), F32)],
     )(decay_cot.T, inputs)
     near, decay_rows = lax.optimization_barrier((near, decay_rows))
     far = lax.ppermute(near, "c", SWAP)
     quarter = call(
         project_body,
-        shape((136, 768), BF),
+        shape((144, 768), BF),
         4,
         2 * 768 * D * 128,
         4 << 20,
@@ -260,13 +239,11 @@
             3,
             2 * 768 * 256 * 512,
             2 << 20,
-            [pltpu.VMEM((ROWS, 128), F32)],
+            [pltpu.VMEM((ROWS, 128), F32), pltpu.VMEM((CHIPS * 2, 128), F32)],
         )(projected, values_cot, decay_rows)
 
     peer = lax.ppermute(gradient(0), "c", SWAP)
-    paired = call(
-        pair_body, chunk, 2, 400000, 1 << 20, [pltpu.VMEM((ROWS, 128), F32)]
-    )(gradient(1), peer)
+    paired = call(pair_body, chunk, 2, 400000, 1 << 20)(gradient(1), peer)
     arrived = across(paired)
     rows = call(spread_body, shape((2, 4, 64, 16 * CHUNK), BF), 1, 8 * 2 * 16 * 128 * 256, 1 << 20)(
         projected
@@ -280,8 +257,8 @@
         [
             pltpu.VMEM((16, 128), F32),
             pltpu.VMEM((16, 128), F32),
-            pltpu.VMEM((2 * CHUNK, 128), F32),
             pltpu.VMEM((4 * CHUNK, 128), F32),
+            pltpu.VMEM((8 * CHUNK, 128), F32),
         ],
     )(arrived, lowrank_mean, lowrank_var)
     near = across(ratio)

time: 115 us -> 113 us (0.983)
    broadcast_in_dim x1 -> x0, local copies, waits for them, and re-layouts: 1.48 us -> none  [local(): jnp.broadcast_to(factor, (CHIPS, 16, 128))]
    unnamed x22 -> x24, local copies, waits for them, and re-layouts: 2.67 us -> 3.35 us
    pallas_call x3 -> x4, Pallas kernels: 2.9 us -> 2.58 us  [the longest x1 1.25 us: local(): call(project_body, shape((144, 768), BF), 4, 2 * 768 * D * 128, 4 << 20,...]
where the time goes in v5:
time: 113 us; the launch traced here: 112 us
  blocking collectives  48.4 us (43%)
  starting transfers between devices  36.4 us (32%)
  waiting for transfers between devices  15.7 us (14%)
  Pallas kernels  7.58 us (7%)
  local copies, waits for them, and re-layouts  3.35 us (3%)
    all_to_all x2, blocking collectives, across(): return lax.all_to_all(tiles, PLANE, 0, 0, tiled=True).reshape(ROWS, 128)  36 us
    all_to_all x1, starting transfers between devices, local(): near = lax.all_to_all(copies, PLANE, 0, 0, tiled=True)  17.1 us
    all_gather x1, blocking collectives, local(): projected = lax.all_gather(quarter, 'x')  12.4 us
    ppermute x2, starting transfers between devices, local(): far = lax.ppermute(near, 'c', SWAP)  10.4 us
    all_to_all x1, waiting for transfers between devices, local(): near = lax.all_to_all(copies, PLANE, 0, 0, tiled=True)  9.67 us
    all_to_all x1, starting transfers between devices, local(): squares = lax.all_to_all(squares, ('c', 'x'), 0, 0, tiled=True)  4.66 us
    all_to_all x1, waiting for transfers between devices, local(): squares = lax.all_to_all(squares, ('c', 'x'), 0, 0, tiled=True)  4.37 us
    ppermute x1, starting transfers between devices, local(): peer = lax.ppermute(gradient(0), 'c', SWAP)  4.21 us
  transfers between devices with their start and end apart: 5, of which 4 were waited for; matrix products, arithmetic and copies ran while one was open for 0% of the time, Pallas kernels for 2%

profile of v5, /device:TPU:1, one launch (start us, length us, event | category | flops | bytes accessed | tf_op | source)
XLA Modules:
  0.0 112.2 jit_solution(17979172417690178365)
XLA Ops:
  0.7 0.7 copy-done.8
  1.3 0.7 shard_map.169
  2.1 17.1 %all-to-all-start = ((bf16[64,16,128]{2,1,0:T(8,128)(2,1)}), bf16[64,16,128]{2,1,0:T(8,128)(2,1)S(1)}, u32[]{:S(2)}, u32[]{:S(2)}) async-start(bf16[64,16,128]{2,1,0:T(8,128)(2,1)} %shard_map.169), calls=%async_computation | async-start | bytes 524288 | tf_op jit(solution)/shard_map/all_to_all | solution.py:214
  19.2 1.9 %copy-done = bf16[768,2048]{1,0:T(8,128)(2,1)S(1)} copy-done((bf16[768,2048]{1,0:T(8,128)(2,1)S(1)}, bf16[768,2048]{1,0:T(8,128)(2,1)}, u32[]{:S(2)}) %copy-start) | copy-done | bytes 3145752
  21.1 0.7 copy-done.7
  21.8 0.5 shard_map.170.dec_ref
  22.4 9.7 %all-to-all-done.near_ref = bf16[64,16,128]{2,1,0:T(8,128)(2,1)S(1)} async-done(((bf16[64,16,128]{2,1,0:T(8,128)(2,1)}), bf16[64,16,128]{2,1,0:T(8,128)(2,1)S(1)}, u32[]{:S(2)}, u32[]{:S(2)}) %all-to-all-start) | async-done | bytes 262176 | tf_op jit(solution)/shard_map/all_to_all | solution.py:214
  32.0 5.1 %collective-permute-start = (bf16[64,16,128]{2,1,0:T(8,128)(2,1)S(1)}, bf16[64,16,128]{2,1,0:T(8,128)(2,1)S(1)}, u32[]{:S(2)}, u32[]{:S(2)}) collective-permute-start(bf16[64,16,128]{2,1,0:T(8,128)(2,1)S(1)} %all-to-all-done.near_ref), channel_id=1, source_target_pairs={{0,4},{4,0},{1,5},{5,1},{2,6},{6,2},{3,7},{7,3},{8,12},{12,8},{9,1... | collective-permute-start | bytes 786440 | tf_op jit(solution)/shard_map/ppermute | solution.py:224
  37.1 1.1 %collective-permute-done.far_ref = bf16[64,16,128]{2,1,0:T(8,128)(2,1)S(1)} collective-permute-done((bf16[64,16,128]{2,1,0:T(8,128)(2,1)S(1)}, bf16[64,16,128]{2,1,0:T(8,128)(2,1)S(1)}, u32[]{:S(2)}, u32[]{:S(2)}) %collective-permute-start) | collective-permute-done | bytes 262176 | tf_op jit(solution)/shard_map/ppermute | solution.py:224
  38.3 1.3 %shard_map.171 = bf16[144,768]{1,0:T(8,128)(2,1)S(1)} custom-call(bf16[768,2048]{1,0:T(8,128)(2,1)S(1)} %copy-done.1, bf16[64,16,128]{2,1,0:T(8,128)(2,1)S(1)} %all-to-all-done.near_ref, bf16[64,16,128]{2,1,0:T(8,128)(2,1)S(1)} %collective-permute-done.far_ref, bf16[16,128]{1,0:T(8,128)(2,1)S(1)} %copy-done.9), custom_call_target="tpu_custom_call" | custom-call | flops 402653184 | bytes 4194304 | tf_op jit(solution)/shard_map/pallas_call | solution.py:225
  39.6 12.4 %all-gather = bf16[576,768]{1,0:T(8,128)(2,1)S(1)} all-gather(bf16[144,768]{1,0:T(8,128)(2,1)S(1)} %shard_map.171), channel_id=2, replica_groups=mesh['z'=8,'y'=8,'c'=2,'x'=4] {'x'}, dimensions={0}, use_global_device_ids=true | all-gather | bytes 1105920 | tf_op jit(solution)/shard_map/all_gather | solution.py:233
  52.0 0.7 shard_map.173
  52.7 4.2 %collective-permute-start.1 = (bf16[1152,128]{1,0:T(8,128)(2,1)S(1)}, bf16[1152,128]{1,0:T(8,128)(2,1)S(1)}, u32[]{:S(2)}, u32[]{:S(2)}) collective-permute-start(bf16[1152,128]{1,0:T(8,128)(2,1)S(1)} %shard_map.173), channel_id=1, source_target_pairs={{0,4},{4,0},{1,5},{5,1},{2,6},{6,2},{3,7},{7,3},{8,12},{12,8},{9,1... | collective-permute-start | bytes 884744 | tf_op jit(solution)/shard_map/ppermute | solution.py:245
  56.9 0.7 shard_map.172.own_ref
  57.6 0.5 collective-permute-done.1.peer_ref
  58.2 17.7 %all_to_all.20 = bf16[64,9,2,128]{3,2,1,0:T(2,128)(2,1)S(1)} all-to-all(bf16[64,9,2,128]{3,2,1,0:T(2,128)(2,1)S(1)} %bitcast.20), channel_id=1, replica_groups=mesh['z'=8,'y'=8,'c'=2,'x'=4] {'z','y'}, dimensions={0} | all-to-all | bytes 589824 | tf_op jit(solution)/shard_map/all_to_all | solution.py:211
  75.8 0.7 shard_map.175
  76.5 18.3 %all_to_all.21 = bf16[64,9,2,128]{3,2,1,0:T(2,128)(2,1)S(1)} all-to-all(bf16[64,9,2,128]{3,2,1,0:T(2,128)(2,1)S(1)} %bitcast.22), channel_id=1, replica_groups=mesh['z'=8,'y'=8,'c'=2,'x'=4] {'z','y'}, dimensions={0} | all-to-all | bytes 589824 | tf_op jit(solution)/shard_map/all_to_all | solution.py:211
  94.9 5.3 %collective-permute-start.2 = (bf16[1152,128]{1,0:T(8,128)(2,1)S(1)}, bf16[1152,128]{1,0:T(8,128)(2,1)S(1)}, u32[]{:S(2)}, u32[]{:S(2)}) collective-permute-start(bf16[1152,128]{1,0:T(8,128)(2,1)S(1)} %bitcast.16), channel_id=1, source_target_pairs={{0,4},{4,0},{1,5},{5,1},{2,6},{6,2},{3,7},{7,3},{8,12},{12,8},{9,1... | collective-permute-start | bytes 884744 | tf_op jit(solution)/shard_map/ppermute | solution.py:265
  100.2 0.7 shard_map.176
  100.9 4.7 %all-to-all-start.3 = ((f32[8,8,128]{2,1,0:T(8,128)}), f32[8,8,128]{2,1,0:T(8,128)S(1)}, u32[]{:S(2)}, u32[]{:S(2)}) async-start(f32[8,8,128]{2,1,0:T(8,128)} %shard_map.176), calls=%async_computation.3 | async-start | bytes 65536 | tf_op jit(solution)/shard_map/all_to_all | solution.py:276
  106.1 4.4 %all-to-all-done.3.squares_ref = f32[8,8,128]{2,1,0:T(8,128)S(1)} async-done(((f32[8,8,128]{2,1,0:T(8,128)}), f32[8,8,128]{2,1,0:T(8,128)S(1)}, u32[]{:S(2)}, u32[]{:S(2)}) %all-to-all-start.3) | async-done | bytes 32800 | tf_op jit(solution)/shard_map/all_to_all | solution.py:276
  110.5 0.8 shard_map.179
  111.3 0.9 shard_map.180
  (25 shorter events, 0.7 us)
Async XLA Ops:
  0.6 0.7 copy-start.8
  1.3 36.9 %copy-start.9 = (bf16[16,128]{1,0:T(8,128)(2,1)S(1)}, bf16[16,128]{1,0:T(8,128)(2,1)}, u32[]{:S(2)}) copy-start(bf16[16,128]{1,0:T(8,128)(2,1)} %own_ref.3) | copy-start | bytes 12292
  2.1 30.0 %all-to-all-start = ((bf16[64,16,128]{2,1,0:T(8,128)(2,1)}), bf16[64,16,128]{2,1,0:T(8,128)(2,1)S(1)}, u32[]{:S(2)}, u32[]{:S(2)}) async-start(bf16[64,16,128]{2,1,0:T(8,128)(2,1)} %shard_map.169), calls=%async_computation | async-start | bytes 524288 | tf_op jit(solution)/shard_map/all_to_all | solution.py:214
  19.2 1.9 %copy-start = (bf16[768,2048]{1,0:T(8,128)(2,1)S(1)}, bf16[768,2048]{1,0:T(8,128)(2,1)}, u32[]{:S(2)}) copy-start(bf16[768,2048]{1,0:T(8,128)(2,1)} %x_ref.3) | copy-start | bytes 9437188
  21.1 0.7 copy-start.7
  21.8 16.5 %copy-start.1 = (bf16[768,2048]{1,0:T(8,128)(2,1)S(1)}, bf16[768,2048]{1,0:T(8,128)(2,1)}, u32[]{:S(2)}) copy-start(bf16[768,2048]{1,0:T(8,128)(2,1)} %x_ref.3) | copy-start | bytes 9437188
  32.0 19.9 %copy-start.2 = (bf16[768,512]{1,0:T(8,128)(2,1)S(1)}, bf16[768,512]{1,0:T(8,128)(2,1)}, u32[]{:S(2)}) copy-start(bf16[768,512]{1,0:T(8,128)(2,1)} %v_ref.3) | copy-start | bytes 2359300
  32.0 6.2 %collective-permute-start = (bf16[64,16,128]{2,1,0:T(8,128)(2,1)S(1)}, bf16[64,16,128]{2,1,0:T(8,128)(2,1)S(1)}, u32[]{:S(2)}, u32[]{:S(2)}) collective-permute-start(bf16[64,16,128]{2,1,0:T(8,128)(2,1)S(1)} %all-to-all-done.near_ref), channel_id=1, source_target_pairs={{0,4},{4,0},{1,5},{5,1},{2,6},{6,2},{3,7},{7,3},{8,12},{12,8},{9,1... | collective-permute-start | bytes 786440 | tf_op jit(solution)/shard_map/ppermute | solution.py:224
  39.5 36.3 %copy-start.10 = (f32[4,512]{1,0:T(4,128)S(1)}, f32[4,512]{1,0:T(4,128)}, u32[]{:S(2)}) copy-start(f32[4,512]{1,0:T(4,128)} %mean_ref.1) | copy-start | bytes 24580
  39.5 36.3 %copy-start.11 = (f32[4,512]{1,0:T(4,128)S(1)}, f32[4,512]{1,0:T(4,128)}, u32[]{:S(2)}) copy-start(f32[4,512]{1,0:T(4,128)} %var_ref.1) | copy-start | bytes 24580
  52.7 57.8 %copy-start.6 = (f32[16,512]{1,0:T(8,128)S(1)}, f32[16,512]{1,0:T(8,128)}, u32[]{:S(2)}) copy-start(f32[16,512]{1,0:T(8,128)} %weight_ref.1) | copy-start | bytes 98308
  52.7 58.6 %copy-start.3 = (f32[2048,16]{0,1:T(8,128)S(1)}, f32[2048,16]{0,1:T(8,128)}, u32[]{:S(2)}) copy-start(f32[2048,16]{0,1:T(8,128)} %param.17) | copy-start | bytes 393220
  52.7 58.6 %copy-start.4 = (f32[2048,16]{0,1:T(8,128)S(1)}, f32[2048,16]{0,1:T(8,128)}, u32[]{:S(2)}) copy-start(f32[2048,16]{0,1:T(8,128)} %param.18) | copy-start | bytes 393220
  52.7 58.6 %copy-start.5 = (f32[2048,16]{0,1:T(8,128)S(1)}, f32[2048,16]{0,1:T(8,128)}, u32[]{:S(2)}) copy-start(f32[2048,16]{0,1:T(8,128)} %param.19) | copy-start | bytes 393220
  52.7 5.4 %collective-permute-start.1 = (bf16[1152,128]{1,0:T(8,128)(2,1)S(1)}, bf16[1152,128]{1,0:T(8,128)(2,1)S(1)}, u32[]{:S(2)}, u32[]{:S(2)}) collective-permute-start(bf16[1152,128]{1,0:T(8,128)(2,1)S(1)} %shard_map.173), channel_id=1, source_target_pairs={{0,4},{4,0},{1,5},{5,1},{2,6},{6,2},{3,7},{7,3},{8,12},{12,8},{9,1... | collective-permute-start | bytes 884744 | tf_op jit(solution)/shard_map/ppermute | solution.py:245
  94.9 11.0 %collective-permute-start.2 = (bf16[1152,128]{1,0:T(8,128)(2,1)S(1)}, bf16[1152,128]{1,0:T(8,128)(2,1)S(1)}, u32[]{:S(2)}, u32[]{:S(2)}) collective-permute-start(bf16[1152,128]{1,0:T(8,128)(2,1)S(1)} %bitcast.16), channel_id=1, source_target_pairs={{0,4},{4,0},{1,5},{5,1},{2,6},{6,2},{3,7},{7,3},{8,12},{12,8},{9,1... | collective-permute-start | bytes 884744 | tf_op jit(solution)/shard_map/ppermute | solution.py:265
  100.9 9.6 %all-to-all-start.3 = ((f32[8,8,128]{2,1,0:T(8,128)}), f32[8,8,128]{2,1,0:T(8,128)S(1)}, u32[]{:S(2)}, u32[]{:S(2)}) async-start(f32[8,8,128]{2,1,0:T(8,128)} %shard_map.176), calls=%async_computation.3 | async-start | bytes 65536 | tf_op jit(solution)/shard_map/all_to_all | solution.py:276

commit v6 on v5

--- a/solution.py
+++ b/solution.py
@@ -145,8 +145,23 @@
 
 
 def decay_update_body(
-    near_ref, far_ref, weight_ref, mean_ref, var_ref, new_out, copy_out, mean_out, var_out, rows
+    near_ref,
+    far_ref,
+    weight_ref,
+    mean_ref,
+    var_ref,
+    low_mean_ref,
+    low_var_ref,
+    new_out,
+    copy_out,
+    mean_out,
+    var_out,
+    low_mean_out,
+    low_var_out,
+    rows,
 ):
+    low_mean_out[...] = low_mean_ref[...]
+    low_var_out[...] = low_var_ref[...]
     core = lax.axis_index("c")
     rows[core] = near_ref[...].astype(F32)
     rows[1 - core] = far_ref[...].astype(F32)
@@ -169,8 +184,8 @@
     row = lax.broadcasted_iota(jnp.int32, (4 * CHUNK, 128), 0)
     row = row - ((row * 3641) >> 16) * CHUNK
     sums = jnp.where(row < 16, jnp.sum(near * near, axis=0), 0.0)
-    sums = jnp.sum(sums.reshape(4 * CHUNK // 8, 8, 128), axis=0)
-    out_ref[...] = jnp.broadcast_to(sums[None], (8, 8, 128))
+    sums = jnp.sum(sums, axis=0, keepdims=True)
+    out_ref[...] = jnp.broadcast_to(sums[None], (8, 1, 128))
 
 
 def product_body(rows_ref, near_ref, far_ref, out_ref):
@@ -242,7 +257,8 @@
             [pltpu.VMEM((ROWS, 128), F32), pltpu.VMEM((CHIPS * 2, 128), F32)],
         )(projected, values_cot, decay_rows)
 
-    peer = lax.ppermute(gradient(0), "c", SWAP)
+    theirs = gradient(0)
+    peer = lax.ppermute(theirs, "c", SWAP)
     paired = call(pair_body, chunk, 2, 400000, 1 << 20)(gradient(1), peer)
     arrived = across(paired)
     rows = call(spread_body, shape((2, 4, 64, 16 * CHUNK), BF), 1, 8 * 2 * 16 * 128 * 256, 1 << 20)(
@@ -250,7 +266,7 @@
     )
     ratio, mean_new, var_new = call(
         moment_body,
-        (chunk, shape((4, 512), F32), shape((4, 512), F32)),
+        (chunk, pltpu.VMEM((4, 512), F32), pltpu.VMEM((4, 512), F32)),
         3,
         400000,
         1 << 20,
@@ -264,15 +280,16 @@
     near = across(ratio)
     far = lax.ppermute(near, "c", SWAP)
     state = shape((H, D), F32)
-    decay_new, decay_copy, decay_mean_new, decay_var_new = call(
+    low = shape((4, 512), F32)
+    (decay_new, decay_copy, decay_mean_new, decay_var_new, mean_new, var_new) = call(
         decay_update_body,
-        (state, shape((H, D), BF), state, state),
-        5,
+        (state, shape((H, D), BF), state, state, low, low),
+        7,
         400000,
         1 << 20,
         [pltpu.VMEM((2, ROWS, 128), F32)],
-    )(near, far, decay_weight.T, decay_mean.T, decay_var.T)
-    squares = call(squares_body, shape((8, 8, 128), F32), 1, 400000, 1 << 20)(near)
+    )(near, far, decay_weight.T, decay_mean.T, decay_var.T, mean_new, var_new)
+    squares = call(squares_body, shape((8, 1, 128), F32), 1, 400000, 1 << 20)(near)
     squares = lax.all_to_all(squares, ("c", "x"), 0, 0, tiled=True)
     delta = call(
         product_body, shape((16, 512), F32), 3, 2 * 64 * 2048 * 128, 1 << 20

time: 113 us -> 112 us (level)
  no operation moved by 1% of the time
where the time goes in v6:
time: 112 us; the launch traced here: 111 us
  blocking collectives  48.4 us (43%)
  starting transfers between devices  36.4 us (32%)
  waiting for transfers between devices  15.3 us (14%)
  Pallas kernels  7.01 us (6%)
  local copies, waits for them, and re-layouts  3.35 us (3%)
    all_to_all x2, blocking collectives, across(): return lax.all_to_all(tiles, PLANE, 0, 0, tiled=True).reshape(ROWS, 128)  36 us
    all_to_all x1, starting transfers between devices, local(): near = lax.all_to_all(copies, PLANE, 0, 0, tiled=True)  17.1 us
    all_gather x1, blocking collectives, local(): projected = lax.all_gather(quarter, 'x')  12.4 us
    ppermute x2, starting transfers between devices, local(): far = lax.ppermute(near, 'c', SWAP)  10.4 us
    all_to_all x1, waiting for transfers between devices, local(): near = lax.all_to_all(copies, PLANE, 0, 0, tiled=True)  9.67 us
    all_to_all x1, starting transfers between devices, local(): squares = lax.all_to_all(squares, ('c', 'x'), 0, 0, tiled=True)  4.66 us
    ppermute x1, starting transfers between devices, local(): peer = lax.ppermute(theirs, 'c', SWAP)  4.21 us
    all_to_all x1, waiting for transfers between devices, local(): squares = lax.all_to_all(squares, ('c', 'x'), 0, 0, tiled=True)  3.97 us
  transfers between devices with their start and end apart: 5, of which 4 were waited for; matrix products, arithmetic and copies ran while one was open for 0% of the time, Pallas kernels for 2%

profile of v6, /device:TPU:1, one launch (start us, length us, event | category | flops | bytes accessed | tf_op | source)
XLA Modules:
  0.0 111.3 jit_solution(18217389978860498952)
XLA Ops:
  0.7 0.7 copy-done.8
  1.3 0.7 shard_map.169
  2.1 17.1 %all-to-all-start = ((bf16[64,16,128]{2,1,0:T(8,128)(2,1)}), bf16[64,16,128]{2,1,0:T(8,128)(2,1)S(1)}, u32[]{:S(2)}, u32[]{:S(2)}) async-start(bf16[64,16,128]{2,1,0:T(8,128)(2,1)} %shard_map.169), calls=%async_computation | async-start | bytes 524288 | tf_op jit(solution)/shard_map/all_to_all | solution.py:229
  19.2 1.9 %copy-done = bf16[768,2048]{1,0:T(8,128)(2,1)S(1)} copy-done((bf16[768,2048]{1,0:T(8,128)(2,1)S(1)}, bf16[768,2048]{1,0:T(8,128)(2,1)}, u32[]{:S(2)}) %copy-start) | copy-done | bytes 3145752
  21.1 0.7 copy-done.7
  21.8 0.5 shard_map.170.dec_ref
  22.4 9.7 %all-to-all-done.near_ref = bf16[64,16,128]{2,1,0:T(8,128)(2,1)S(1)} async-done(((bf16[64,16,128]{2,1,0:T(8,128)(2,1)}), bf16[64,16,128]{2,1,0:T(8,128)(2,1)S(1)}, u32[]{:S(2)}, u32[]{:S(2)}) %all-to-all-start) | async-done | bytes 262176 | tf_op jit(solution)/shard_map/all_to_all | solution.py:229
  32.0 5.1 %collective-permute-start = (bf16[64,16,128]{2,1,0:T(8,128)(2,1)S(1)}, bf16[64,16,128]{2,1,0:T(8,128)(2,1)S(1)}, u32[]{:S(2)}, u32[]{:S(2)}) collective-permute-start(bf16[64,16,128]{2,1,0:T(8,128)(2,1)S(1)} %all-to-all-done.near_ref), channel_id=1, source_target_pairs={{0,4},{4,0},{1,5},{5,1},{2,6},{6,2},{3,7},{7,3},{8,12},{12,8},{9,1... | collective-permute-start | bytes 786440 | tf_op jit(solution)/shard_map/ppermute | solution.py:239
  37.1 1.1 %collective-permute-done.far_ref = bf16[64,16,128]{2,1,0:T(8,128)(2,1)S(1)} collective-permute-done((bf16[64,16,128]{2,1,0:T(8,128)(2,1)S(1)}, bf16[64,16,128]{2,1,0:T(8,128)(2,1)S(1)}, u32[]{:S(2)}, u32[]{:S(2)}) %collective-permute-start) | collective-permute-done | bytes 262176 | tf_op jit(solution)/shard_map/ppermute | solution.py:239
  38.3 1.3 %shard_map.171 = bf16[144,768]{1,0:T(8,128)(2,1)S(1)} custom-call(bf16[768,2048]{1,0:T(8,128)(2,1)S(1)} %copy-done.1, bf16[64,16,128]{2,1,0:T(8,128)(2,1)S(1)} %all-to-all-done.near_ref, bf16[64,16,128]{2,1,0:T(8,128)(2,1)S(1)} %collective-permute-done.far_ref, bf16[16,128]{1,0:T(8,128)(2,1)S(1)} %copy-done.9), custom_call_target="tpu_custom_call" | custom-call | flops 402653184 | bytes 4194304 | tf_op jit(solution)/shard_map/pallas_call | solution.py:240
  39.6 12.4 %all-gather = bf16[576,768]{1,0:T(8,128)(2,1)S(1)} all-gather(bf16[144,768]{1,0:T(8,128)(2,1)S(1)} %shard_map.171), channel_id=2, replica_groups=mesh['z'=8,'y'=8,'c'=2,'x'=4] {'x'}, dimensions={0}, use_global_device_ids=true | all-gather | bytes 1105920 | tf_op jit(solution)/shard_map/all_gather | solution.py:248
  52.0 0.7 shard_map.173
  52.7 4.2 %collective-permute-start.1 = (bf16[1152,128]{1,0:T(8,128)(2,1)S(1)}, bf16[1152,128]{1,0:T(8,128)(2,1)S(1)}, u32[]{:S(2)}, u32[]{:S(2)}) collective-permute-start(bf16[1152,128]{1,0:T(8,128)(2,1)S(1)} %shard_map.173), channel_id=1, source_target_pairs={{0,4},{4,0},{1,5},{5,1},{2,6},{6,2},{3,7},{7,3},{8,12},{12,8},{9,1... | collective-permute-start | bytes 884744 | tf_op jit(solution)/shard_map/ppermute | solution.py:261
  56.9 0.7 shard_map.172.own_ref
  57.6 0.5 collective-permute-done.1.peer_ref
  58.2 17.7 %all_to_all.20 = bf16[64,9,2,128]{3,2,1,0:T(2,128)(2,1)S(1)} all-to-all(bf16[64,9,2,128]{3,2,1,0:T(2,128)(2,1)S(1)} %bitcast.20), channel_id=1, replica_groups=mesh['z'=8,'y'=8,'c'=2,'x'=4] {'z','y'}, dimensions={0} | all-to-all | bytes 589824 | tf_op jit(solution)/shard_map/all_to_all | solution.py:226
  76.0 18.4 %all_to_all.21 = bf16[64,9,2,128]{3,2,1,0:T(2,128)(2,1)S(1)} all-to-all(bf16[64,9,2,128]{3,2,1,0:T(2,128)(2,1)S(1)} %bitcast.22), channel_id=1, replica_groups=mesh['z'=8,'y'=8,'c'=2,'x'=4] {'z','y'}, dimensions={0} | all-to-all | bytes 589824 | tf_op jit(solution)/shard_map/all_to_all | solution.py:226
  94.3 5.3 %collective-permute-start.2 = (bf16[1152,128]{1,0:T(8,128)(2,1)S(1)}, bf16[1152,128]{1,0:T(8,128)(2,1)S(1)}, u32[]{:S(2)}, u32[]{:S(2)}) collective-permute-start(bf16[1152,128]{1,0:T(8,128)(2,1)S(1)} %bitcast.16), channel_id=1, source_target_pairs={{0,4},{4,0},{1,5},{5,1},{2,6},{6,2},{3,7},{7,3},{8,12},{12,8},{9,1... | collective-permute-start | bytes 884744 | tf_op jit(solution)/shard_map/ppermute | solution.py:281
  99.6 0.7 shard_map.176
  100.3 4.7 %all-to-all-start.3 = ((f32[8,1,128]{2,1,0:T(1,128)}), f32[8,1,128]{2,1,0:T(1,128)S(1)}, u32[]{:S(2)}, u32[]{:S(2)}) async-start(f32[8,1,128]{2,1,0:T(1,128)} %shard_map.176), calls=%async_computation.3 | async-start | bytes 8192 | tf_op jit(solution)/shard_map/all_to_all | solution.py:293
  105.0 0.3 shard_map.177.rows_ref
  105.5 4.0 %all-to-all-done.3.squares_ref = f32[8,1,128]{2,1,0:T(1,128)S(1)} async-done(((f32[8,1,128]{2,1,0:T(1,128)}), f32[8,1,128]{2,1,0:T(1,128)S(1)}, u32[]{:S(2)}, u32[]{:S(2)}) %all-to-all-start.3) | async-done | bytes 4128 | tf_op jit(solution)/shard_map/all_to_all | solution.py:293
  109.5 0.8 shard_map.179
  110.3 0.9 shard_map.180
  (25 shorter events, 0.5 us)
Async XLA Ops:
  0.6 0.7 copy-start.8
  1.3 36.9 %copy-start.9 = (bf16[16,128]{1,0:T(8,128)(2,1)S(1)}, bf16[16,128]{1,0:T(8,128)(2,1)}, u32[]{:S(2)}) copy-start(bf16[16,128]{1,0:T(8,128)(2,1)} %own_ref.3) | copy-start | bytes 12292
  2.1 30.0 %all-to-all-start = ((bf16[64,16,128]{2,1,0:T(8,128)(2,1)}), bf16[64,16,128]{2,1,0:T(8,128)(2,1)S(1)}, u32[]{:S(2)}, u32[]{:S(2)}) async-start(bf16[64,16,128]{2,1,0:T(8,128)(2,1)} %shard_map.169), calls=%async_computation | async-start | bytes 524288 | tf_op jit(solution)/shard_map/all_to_all | solution.py:229
  19.2 1.9 %copy-start = (bf16[768,2048]{1,0:T(8,128)(2,1)S(1)}, bf16[768,2048]{1,0:T(8,128)(2,1)}, u32[]{:S(2)}) copy-start(bf16[768,2048]{1,0:T(8,128)(2,1)} %x_ref.3) | copy-start | bytes 9437188
  21.1 0.7 copy-start.7
  21.8 16.5 %copy-start.1 = (bf16[768,2048]{1,0:T(8,128)(2,1)S(1)}, bf16[768,2048]{1,0:T(8,128)(2,1)}, u32[]{:S(2)}) copy-start(bf16[768,2048]{1,0:T(8,128)(2,1)} %x_ref.3) | copy-start | bytes 9437188
  32.0 19.9 %copy-start.2 = (bf16[768,512]{1,0:T(8,128)(2,1)S(1)}, bf16[768,512]{1,0:T(8,128)(2,1)}, u32[]{:S(2)}) copy-start(bf16[768,512]{1,0:T(8,128)(2,1)} %v_ref.3) | copy-start | bytes 2359300
  32.0 6.2 %collective-permute-start = (bf16[64,16,128]{2,1,0:T(8,128)(2,1)S(1)}, bf16[64,16,128]{2,1,0:T(8,128)(2,1)S(1)}, u32[]{:S(2)}, u32[]{:S(2)}) collective-permute-start(bf16[64,16,128]{2,1,0:T(8,128)(2,1)S(1)} %all-to-all-done.near_ref), channel_id=1, source_target_pairs={{0,4},{4,0},{1,5},{5,1},{2,6},{6,2},{3,7},{7,3},{8,12},{12,8},{9,1... | collective-permute-start | bytes 786440 | tf_op jit(solution)/shard_map/ppermute | solution.py:239
  39.5 36.3 %copy-start.10 = (f32[4,512]{1,0:T(4,128)S(1)}, f32[4,512]{1,0:T(4,128)}, u32[]{:S(2)}) copy-start(f32[4,512]{1,0:T(4,128)} %mean_ref.1) | copy-start | bytes 24580
  39.5 36.3 %copy-start.11 = (f32[4,512]{1,0:T(4,128)S(1)}, f32[4,512]{1,0:T(4,128)}, u32[]{:S(2)}) copy-start(f32[4,512]{1,0:T(4,128)} %var_ref.1) | copy-start | bytes 24580
  52.7 56.8 %copy-start.6 = (f32[16,512]{1,0:T(8,128)S(1)}, f32[16,512]{1,0:T(8,128)}, u32[]{:S(2)}) copy-start(f32[16,512]{1,0:T(8,128)} %weight_ref.1) | copy-start | bytes 98308
  52.7 57.7 %copy-start.3 = (f32[2048,16]{0,1:T(8,128)S(1)}, f32[2048,16]{0,1:T(8,128)}, u32[]{:S(2)}) copy-start(f32[2048,16]{0,1:T(8,128)} %param.17) | copy-start | bytes 393220
  52.7 57.7 %copy-start.4 = (f32[2048,16]{0,1:T(8,128)S(1)}, f32[2048,16]{0,1:T(8,128)}, u32[]{:S(2)}) copy-start(f32[2048,16]{0,1:T(8,128)} %param.18) | copy-start | bytes 393220
  52.7 57.6 %copy-start.5 = (f32[2048,16]{0,1:T(8,128)S(1)}, f32[2048,16]{0,1:T(8,128)}, u32[]{:S(2)}) copy-start(f32[2048,16]{0,1:T(8,128)} %param.19) | copy-start | bytes 393220
  52.7 5.4 %collective-permute-start.1 = (bf16[1152,128]{1,0:T(8,128)(2,1)S(1)}, bf16[1152,128]{1,0:T(8,128)(2,1)S(1)}, u32[]{:S(2)}, u32[]{:S(2)}) collective-permute-start(bf16[1152,128]{1,0:T(8,128)(2,1)S(1)} %shard_map.173), channel_id=1, source_target_pairs={{0,4},{4,0},{1,5},{5,1},{2,6},{6,2},{3,7},{7,3},{8,12},{12,8},{9,1... | collective-permute-start | bytes 884744 | tf_op jit(solution)/shard_map/ppermute | solution.py:261
  94.3 10.9 %collective-permute-start.2 = (bf16[1152,128]{1,0:T(8,128)(2,1)S(1)}, bf16[1152,128]{1,0:T(8,128)(2,1)S(1)}, u32[]{:S(2)}, u32[]{:S(2)}) collective-permute-start(bf16[1152,128]{1,0:T(8,128)(2,1)S(1)} %bitcast.16), channel_id=1, source_target_pairs={{0,4},{4,0},{1,5},{5,1},{2,6},{6,2},{3,7},{7,3},{8,12},{12,8},{9,1... | collective-permute-start | bytes 884744 | tf_op jit(solution)/shard_map/ppermute | solution.py:281
  100.3 9.2 %all-to-all-start.3 = ((f32[8,1,128]{2,1,0:T(1,128)}), f32[8,1,128]{2,1,0:T(1,128)S(1)}, u32[]{:S(2)}, u32[]{:S(2)}) async-start(f32[8,1,128]{2,1,0:T(1,128)} %shard_map.176), calls=%async_computation.3 | async-start | bytes 8192 | tf_op jit(solution)/shard_map/all_to_all | solution.py:293

commit v7 on v6

--- a/solution.py
+++ b/solution.py
@@ -63,8 +63,9 @@
         order, part, (((1,), (1,)), ((), ())), preferred_element_type=F32
     ).astype(BF)
     out_ref[0:128, :] = turned
-    out_ref[128:144, :] = jnp.zeros((16, 768), BF)
-    out_ref[128:144, 0:128] = own_ref[...]
+    out_ref[128:136, :] = jnp.zeros((8, 768), BF)
+    out_ref[128:136, 0:128] = own_ref[0:8]
+    out_ref[128:136, 128:256] = own_ref[8:16]
 
 
 def gradient_body(half, p_ref, v_ref, dec_ref, out_ref, rows, dec):
@@ -137,7 +138,13 @@
         hit = (lane == chip * 8 + half * 4 + (row & 3)) & (row < 16)
         pick = jnp.where(hit, 1.0, 0.0).astype(BF)
         for q in range(4):
-            rows = jnp.dot(p_ref[q, 128:144, 0:128], pick, preferred_element_type=F32)
+            own = jnp.concatenate(
+                [
+                    p_ref[q, 128:136, 0:128].astype(F32),
+                    p_ref[q, 128:136, 128:256].astype(F32),
+                ]
+            ).astype(BF)
+            rows = jnp.dot(own, pick, preferred_element_type=F32)
             for cb in range(4):
                 out_ref[side, q, cb * 16 : cb * 16 + 16, :] = jnp.where(
                     column == cb, rows, 0.0
@@ -239,7 +246,7 @@
     far = lax.ppermute(near, "c", SWAP)
     quarter = call(
         project_body,
-        shape((144, 768), BF),
+        shape((136, 768), BF),
         4,
         2 * 768 * D * 128,
         4 << 20,

time: 112 us -> 112 us (level)
  no operation moved by 1% of the time
where the time goes in v7:
time: 112 us; the launch traced here: 111 us
  blocking collectives  48.2 us (43%)
  starting transfers between devices  36.3 us (32%)
  waiting for transfers between devices  15.3 us (14%)
  Pallas kernels  7.01 us (6%)
  local copies, waits for them, and re-layouts  3.35 us (3%)
    all_to_all x2, blocking collectives, across(): return lax.all_to_all(tiles, PLANE, 0, 0, tiled=True).reshape(ROWS, 128)  36 us
    all_to_all x1, starting transfers between devices, local(): near = lax.all_to_all(copies, PLANE, 0, 0, tiled=True)  17.1 us
    all_gather x1, blocking collectives, local(): projected = lax.all_gather(quarter, 'x')  12.2 us
    ppermute x2, starting transfers between devices, local(): far = lax.ppermute(near, 'c', SWAP)  10.4 us
    all_to_all x1, waiting for transfers between devices, local(): near = lax.all_to_all(copies, PLANE, 0, 0, tiled=True)  9.67 us
    all_to_all x1, starting transfers between devices, local(): squares = lax.all_to_all(squares, ('c', 'x'), 0, 0, tiled=True)  4.55 us
    ppermute x1, starting transfers between devices, local(): peer = lax.ppermute(theirs, 'c', SWAP)  4.25 us
    all_to_all x1, waiting for transfers between devices, local(): squares = lax.all_to_all(squares, ('c', 'x'), 0, 0, tiled=True)  3.97 us
  transfers between devices with their start and end apart: 5, of which 4 were waited for; matrix products, arithmetic and copies ran while one was open for 0% of the time, Pallas kernels for 2%

profile of v7, /device:TPU:1, one launch (start us, length us, event | category | flops | bytes accessed | tf_op | source)
XLA Modules:
  0.0 111.0 jit_solution(6128372675504316295)
XLA Ops:
  0.7 0.7 copy-done.8
  1.3 0.7 shard_map.169
  2.1 17.1 %all-to-all-start = ((bf16[64,16,128]{2,1,0:T(8,128)(2,1)}), bf16[64,16,128]{2,1,0:T(8,128)(2,1)S(1)}, u32[]{:S(2)}, u32[]{:S(2)}) async-start(bf16[64,16,128]{2,1,0:T(8,128)(2,1)} %shard_map.169), calls=%async_computation | async-start | bytes 524288 | tf_op jit(solution)/shard_map/all_to_all | solution.py:236
  19.2 1.9 %copy-done = bf16[768,2048]{1,0:T(8,128)(2,1)S(1)} copy-done((bf16[768,2048]{1,0:T(8,128)(2,1)S(1)}, bf16[768,2048]{1,0:T(8,128)(2,1)}, u32[]{:S(2)}) %copy-start) | copy-done | bytes 3145752
  21.1 0.7 copy-done.7
  21.8 0.5 shard_map.170.dec_ref
  22.4 9.7 %all-to-all-done.near_ref = bf16[64,16,128]{2,1,0:T(8,128)(2,1)S(1)} async-done(((bf16[64,16,128]{2,1,0:T(8,128)(2,1)}), bf16[64,16,128]{2,1,0:T(8,128)(2,1)S(1)}, u32[]{:S(2)}, u32[]{:S(2)}) %all-to-all-start) | async-done | bytes 262176 | tf_op jit(solution)/shard_map/all_to_all | solution.py:236
  32.0 5.1 %collective-permute-start = (bf16[64,16,128]{2,1,0:T(8,128)(2,1)S(1)}, bf16[64,16,128]{2,1,0:T(8,128)(2,1)S(1)}, u32[]{:S(2)}, u32[]{:S(2)}) collective-permute-start(bf16[64,16,128]{2,1,0:T(8,128)(2,1)S(1)} %all-to-all-done.near_ref), channel_id=1, source_target_pairs={{0,4},{4,0},{1,5},{5,1},{2,6},{6,2},{3,7},{7,3},{8,12},{12,8},{9,1... | collective-permute-start | bytes 786440 | tf_op jit(solution)/shard_map/ppermute | solution.py:246
  37.1 1.1 %collective-permute-done.far_ref = bf16[64,16,128]{2,1,0:T(8,128)(2,1)S(1)} collective-permute-done((bf16[64,16,128]{2,1,0:T(8,128)(2,1)S(1)}, bf16[64,16,128]{2,1,0:T(8,128)(2,1)S(1)}, u32[]{:S(2)}, u32[]{:S(2)}) %collective-permute-start) | collective-permute-done | bytes 262176 | tf_op jit(solution)/shard_map/ppermute | solution.py:246
  38.3 1.2 %shard_map.171 = bf16[136,768]{1,0:T(8,128)(2,1)S(1)} custom-call(bf16[768,2048]{1,0:T(8,128)(2,1)S(1)} %copy-done.1, bf16[64,16,128]{2,1,0:T(8,128)(2,1)S(1)} %all-to-all-done.near_ref, bf16[64,16,128]{2,1,0:T(8,128)(2,1)S(1)} %collective-permute-done.far_ref, bf16[16,128]{1,0:T(8,128)(2,1)S(1)} %copy-done.9), custom_call_target="tpu_custom_call" | custom-call | flops 402653184 | bytes 4194304 | tf_op jit(solution)/shard_map/pallas_call | solution.py:247
  39.6 12.2 %all-gather = bf16[544,768]{1,0:T(8,128)(2,1)S(1)} all-gather(bf16[136,768]{1,0:T(8,128)(2,1)S(1)} %shard_map.171), channel_id=2, replica_groups=mesh['z'=8,'y'=8,'c'=2,'x'=4] {'x'}, dimensions={0}, use_global_device_ids=true | all-gather | bytes 1044480 | tf_op jit(solution)/shard_map/all_gather | solution.py:255
  51.8 0.7 shard_map.173
  52.5 4.3 %collective-permute-start.1 = (bf16[1152,128]{1,0:T(8,128)(2,1)S(1)}, bf16[1152,128]{1,0:T(8,128)(2,1)S(1)}, u32[]{:S(2)}, u32[]{:S(2)}) collective-permute-start(bf16[1152,128]{1,0:T(8,128)(2,1)S(1)} %shard_map.173), channel_id=1, source_target_pairs={{0,4},{4,0},{1,5},{5,1},{2,6},{6,2},{3,7},{7,3},{8,12},{12,8},{9,1... | collective-permute-start | bytes 884744 | tf_op jit(solution)/shard_map/ppermute | solution.py:268
  56.8 0.7 shard_map.172.own_ref
  57.4 0.5 collective-permute-done.1.peer_ref
  58.0 17.6 %all_to_all.20 = bf16[64,9,2,128]{3,2,1,0:T(2,128)(2,1)S(1)} all-to-all(bf16[64,9,2,128]{3,2,1,0:T(2,128)(2,1)S(1)} %bitcast.20), channel_id=1, replica_groups=mesh['z'=8,'y'=8,'c'=2,'x'=4] {'z','y'}, dimensions={0} | all-to-all | bytes 589824 | tf_op jit(solution)/shard_map/all_to_all | solution.py:233
  75.8 18.3 %all_to_all.21 = bf16[64,9,2,128]{3,2,1,0:T(2,128)(2,1)S(1)} all-to-all(bf16[64,9,2,128]{3,2,1,0:T(2,128)(2,1)S(1)} %bitcast.22), channel_id=1, replica_groups=mesh['z'=8,'y'=8,'c'=2,'x'=4] {'z','y'}, dimensions={0} | all-to-all | bytes 589824 | tf_op jit(solution)/shard_map/all_to_all | solution.py:233
  94.1 5.3 %collective-permute-start.2 = (bf16[1152,128]{1,0:T(8,128)(2,1)S(1)}, bf16[1152,128]{1,0:T(8,128)(2,1)S(1)}, u32[]{:S(2)}, u32[]{:S(2)}) collective-permute-start(bf16[1152,128]{1,0:T(8,128)(2,1)S(1)} %bitcast.16), channel_id=1, source_target_pairs={{0,4},{4,0},{1,5},{5,1},{2,6},{6,2},{3,7},{7,3},{8,12},{12,8},{9,1... | collective-permute-start | bytes 884744 | tf_op jit(solution)/shard_map/ppermute | solution.py:288
  99.4 0.7 shard_map.176
  100.1 4.6 %all-to-all-start.3 = ((f32[8,1,128]{2,1,0:T(1,128)}), f32[8,1,128]{2,1,0:T(1,128)S(1)}, u32[]{:S(2)}, u32[]{:S(2)}) async-start(f32[8,1,128]{2,1,0:T(1,128)} %shard_map.176), calls=%async_computation.3 | async-start | bytes 8192 | tf_op jit(solution)/shard_map/all_to_all | solution.py:300
  104.7 0.3 shard_map.177.rows_ref
  105.2 4.0 %all-to-all-done.3.squares_ref = f32[8,1,128]{2,1,0:T(1,128)S(1)} async-done(((f32[8,1,128]{2,1,0:T(1,128)}), f32[8,1,128]{2,1,0:T(1,128)S(1)}, u32[]{:S(2)}, u32[]{:S(2)}) %all-to-all-start.3) | async-done | bytes 4128 | tf_op jit(solution)/shard_map/all_to_all | solution.py:300
  109.2 0.8 shard_map.179
  110.1 0.9 shard_map.180
  (25 shorter events, 0.5 us)
Async XLA Ops:
  0.6 0.7 copy-start.8
  1.3 36.9 %copy-start.9 = (bf16[16,128]{1,0:T(8,128)(2,1)S(1)}, bf16[16,128]{1,0:T(8,128)(2,1)}, u32[]{:S(2)}) copy-start(bf16[16,128]{1,0:T(8,128)(2,1)} %own_ref.3) | copy-start | bytes 12292
  2.1 30.0 %all-to-all-start = ((bf16[64,16,128]{2,1,0:T(8,128)(2,1)}), bf16[64,16,128]{2,1,0:T(8,128)(2,1)S(1)}, u32[]{:S(2)}, u32[]{:S(2)}) async-start(bf16[64,16,128]{2,1,0:T(8,128)(2,1)} %shard_map.169), calls=%async_computation | async-start | bytes 524288 | tf_op jit(solution)/shard_map/all_to_all | solution.py:236
  19.2 1.9 %copy-start = (bf16[768,2048]{1,0:T(8,128)(2,1)S(1)}, bf16[768,2048]{1,0:T(8,128)(2,1)}, u32[]{:S(2)}) copy-start(bf16[768,2048]{1,0:T(8,128)(2,1)} %x_ref.3) | copy-start | bytes 9437188
  21.1 0.7 copy-start.7
  21.8 16.5 %copy-start.1 = (bf16[768,2048]{1,0:T(8,128)(2,1)S(1)}, bf16[768,2048]{1,0:T(8,128)(2,1)}, u32[]{:S(2)}) copy-start(bf16[768,2048]{1,0:T(8,128)(2,1)} %x_ref.3) | copy-start | bytes 9437188
  32.0 19.7 %copy-start.2 = (bf16[768,512]{1,0:T(8,128)(2,1)S(1)}, bf16[768,512]{1,0:T(8,128)(2,1)}, u32[]{:S(2)}) copy-start(bf16[768,512]{1,0:T(8,128)(2,1)} %v_ref.3) | copy-start | bytes 2359300
  32.0 6.2 %collective-permute-start = (bf16[64,16,128]{2,1,0:T(8,128)(2,1)S(1)}, bf16[64,16,128]{2,1,0:T(8,128)(2,1)S(1)}, u32[]{:S(2)}, u32[]{:S(2)}) collective-permute-start(bf16[64,16,128]{2,1,0:T(8,128)(2,1)S(1)} %all-to-all-done.near_ref), channel_id=1, source_target_pairs={{0,4},{4,0},{1,5},{5,1},{2,6},{6,2},{3,7},{7,3},{8,12},{12,8},{9,1... | collective-permute-start | bytes 786440 | tf_op jit(solution)/shard_map/ppermute | solution.py:246
  39.5 36.1 %copy-start.10 = (f32[4,512]{1,0:T(4,128)S(1)}, f32[4,512]{1,0:T(4,128)}, u32[]{:S(2)}) copy-start(f32[4,512]{1,0:T(4,128)} %mean_ref.1) | copy-start | bytes 24580
  39.5 36.1 %copy-start.11 = (f32[4,512]{1,0:T(4,128)S(1)}, f32[4,512]{1,0:T(4,128)}, u32[]{:S(2)}) copy-start(f32[4,512]{1,0:T(4,128)} %var_ref.1) | copy-start | bytes 24580
  52.4 56.8 %copy-start.6 = (f32[16,512]{1,0:T(8,128)S(1)}, f32[16,512]{1,0:T(8,128)}, u32[]{:S(2)}) copy-start(f32[16,512]{1,0:T(8,128)} %weight_ref.1) | copy-start | bytes 98308
  52.5 57.6 %copy-start.3 = (f32[2048,16]{0,1:T(8,128)S(1)}, f32[2048,16]{0,1:T(8,128)}, u32[]{:S(2)}) copy-start(f32[2048,16]{0,1:T(8,128)} %param.17) | copy-start | bytes 393220
  52.5 57.6 %copy-start.4 = (f32[2048,16]{0,1:T(8,128)S(1)}, f32[2048,16]{0,1:T(8,128)}, u32[]{:S(2)}) copy-start(f32[2048,16]{0,1:T(8,128)} %param.18) | copy-start | bytes 393220
  52.5 57.6 %copy-start.5 = (f32[2048,16]{0,1:T(8,128)S(1)}, f32[2048,16]{0,1:T(8,128)}, u32[]{:S(2)}) copy-start(f32[2048,16]{0,1:T(8,128)} %param.19) | copy-start | bytes 393220
  52.5 5.4 %collective-permute-start.1 = (bf16[1152,128]{1,0:T(8,128)(2,1)S(1)}, bf16[1152,128]{1,0:T(8,128)(2,1)S(1)}, u32[]{:S(2)}, u32[]{:S(2)}) collective-permute-start(bf16[1152,128]{1,0:T(8,128)(2,1)S(1)} %shard_map.173), channel_id=1, source_target_pairs={{0,4},{4,0},{1,5},{5,1},{2,6},{6,2},{3,7},{7,3},{8,12},{12,8},{9,1... | collective-permute-start | bytes 884744 | tf_op jit(solution)/shard_map/ppermute | solution.py:268
  94.1 10.9 %collective-permute-start.2 = (bf16[1152,128]{1,0:T(8,128)(2,1)S(1)}, bf16[1152,128]{1,0:T(8,128)(2,1)S(1)}, u32[]{:S(2)}, u32[]{:S(2)}) collective-permute-start(bf16[1152,128]{1,0:T(8,128)(2,1)S(1)} %bitcast.16), channel_id=1, source_target_pairs={{0,4},{4,0},{1,5},{5,1},{2,6},{6,2},{3,7},{7,3},{8,12},{12,8},{9,1... | collective-permute-start | bytes 884744 | tf_op jit(solution)/shard_map/ppermute | solution.py:288
  100.1 9.1 %all-to-all-start.3 = ((f32[8,1,128]{2,1,0:T(1,128)}), f32[8,1,128]{2,1,0:T(1,128)S(1)}, u32[]{:S(2)}, u32[]{:S(2)}) async-start(f32[8,1,128]{2,1,0:T(1,128)} %shard_map.176), calls=%async_computation.3 | async-start | bytes 8192 | tf_op jit(solution)/shard_map/all_to_all | solution.py:300
